TPU v7x, 128 devices: a whole 4x4x4 slice. The times are simulated.
128 devices in a mesh: sp: 64 (over z, y, x), tp: 2 (over core).
Axes of the slice: x: 4, y: 4, z: 4, core: 2. Of those that a mesh axis runs over, the one named last changes fastest.
Arguments:
- queries_small: bfloat16 [16384, 1024], P('sp', 'tp'), may hold values from -160 to 160
- queries_large: bfloat16 [16384, 1024], P('sp', 'tp'), may hold values from -160 to 160
- kv_small: bfloat16 [16384, 128], P('sp'), may hold values from -4 to 4
- kv_large: bfloat16 [16384, 256], P('sp'), may hold values from -4 to 4
- cum_small: float32 [16, 16384], P('tp', 'sp'), may hold values from -2050 to 0, as said below
- cum_large: float32 [8, 16384], P('tp', 'sp'), may hold values from -2050 to 0, as said below
- residual: bfloat16 [16384, 2048], P(('sp', 'tp')), may hold values from -6 to 6
- out_small: bfloat16 [1024, 2048], replicated, may hold values from -0.125 to 0.125
- out_large: bfloat16 [1024, 2048], replicated, may hold values from -0.125 to 0.125
- gain_mix: float32 [2048], replicated, may hold values from 0.1 to 1.9
- gain_route: float32 [2048], replicated, may hold values from 0.1 to 1.9
- gain_blend: float32 [2048], replicated, may hold values from 0.1 to 1.9
- w_gate: bfloat16 [128, 2048, 1024], P(('sp', 'tp')), may hold values from -0.125 to 0.125
- w_up: bfloat16 [128, 2048, 1024], P(('sp', 'tp')), may hold values from -0.125 to 0.125
- w_down: bfloat16 [128, 1024, 2048], P(('sp', 'tp')), may hold values from -0.1875 to 0.1875
- route: int32 [2, 16384], P(None, ('sp', 'tp')), may hold values from 0 to 127, as said below
- route_bias: float32 [16384], P(('sp', 'tp')), may hold values from -6 to 6
Outputs:
- result: bfloat16 [16384, 2048], P(('sp', 'tp'))
Inputs may be any that keep to these rules, and one draw needn't show every extreme that they name: `cum_small`: each row is non-increasing along positions. `cum_large`: each row is non-increasing along positions. route[0, t] and route[1, t] are different experts of the same group of 32 consecutive experts. Among the 128 positions of one device (aligned blocks), no expert is named by more than 4 of them; in every draw all experts of one group are named by exactly 4 positions of every device. Within one device's positions the loads of the experts of one group differ by at most 2.
All inputs are finite; a program needn't handle non-finite values.
Results may differ from a plain program's by a relative error of at most 0.014.
Values may be sent and summed in bfloat16 or wider, within the bound.
A program may use at most 128 MiB of HBM per device.

v0:
```python
import math

import jax
import jax.numpy as jnp
from jax import lax
from jax.sharding import PartitionSpec as P

norm_eps = 1e-06
far_score = -1e30


def sent_to_all(array, axis):
    devices = lax.axis_size(axis)
    return lax.all_to_all(
        jnp.broadcast_to(array[None], (devices, *array.shape)), axis, 0, 0, tiled=True
    )


def laid_out(tiles, dim):
    lengths = list(tiles.shape[1:])
    lengths[dim] *= tiles.shape[0]
    return jnp.moveaxis(tiles, 0, dim).reshape(lengths)


def gathered_copies(array, axis, dim):
    tiles = sent_to_all(array, axis)
    return laid_out(tiles, dim)


def sent_together(arrays, axis, dim, along):
    both = jnp.concatenate(arrays, axis=along)
    out, at, gathered = (gathered_copies(both, axis, dim), 0, [])
    for a in arrays:
        gathered.append(lax.slice_in_dim(out, at, at + a.shape[along], axis=along))
        at += a.shape[along]
    return tuple(gathered)


def sent_together_2(arrays, axis, dim, along):
    widths = [a.shape[along] for a in arrays]
    both = jnp.concatenate(arrays, axis=along)
    out = lax.all_gather(both, axis, axis=dim, tiled=True)
    return tuple(jnp.split(out, [sum(widths[:k]) for k in range(1, len(widths))], axis=along))


def cut_along(array, dim, devices):
    lengths = array.shape
    tiles = array.reshape(*lengths[:dim], devices, lengths[dim] // devices, *lengths[dim + 1 :])
    return jnp.moveaxis(tiles, dim, 0)


def sum_at_owner(array, axis, dim):
    devices = lax.axis_size(axis)
    tiles = lax.all_to_all(cut_along(array, dim, devices), axis, 0, 0, tiled=True)
    return jnp.sum(tiles.astype(jnp.float32), axis=0)


def rms_scale(values, gain_row):
    return (
        values * lax.rsqrt(jnp.mean(values * values, axis=-1, keepdims=True) + norm_eps) * gain_row
    )


def online_update(carried, queries, query_cum, keys_values, key_cum, key_pos, query_pos):
    running_max, running_sum, weighted = carried
    head_size = keys_values.shape[1] // 2
    key_rows = keys_values[:, :head_size]
    value_rows = keys_values[:, head_size:]
    scores = jnp.einsum(
        "qhd,kd->hqk", queries, key_rows, preferred_element_type=jnp.float32
    ) * head_size ** (-0.5)
    scores = scores + query_cum[:, :, None] - key_cum[:, None, :]
    allowed = key_pos[None, None, :] <= query_pos[None, :, None]
    scores = jnp.where(allowed, scores, far_score)
    newest = jnp.maximum(running_max, jnp.max(scores, axis=-1))
    weights = jnp.where(allowed, jnp.exp(scores - newest[:, :, None]), 0.0)
    factor = jnp.exp(running_max - newest)
    running_sum = running_sum * factor + jnp.sum(weights, axis=-1)
    weighted = weighted * factor[:, :, None] + jnp.einsum(
        "hqk,kd->hqd", weights.astype(jnp.bfloat16), value_rows, preferred_element_type=jnp.float32
    )
    return (newest, running_sum, weighted)


def attend_keys(
    softmax_state,
    query_small,
    query_large,
    qcum_small,
    qcum_large,
    query_pos,
    part_small,
    part_large,
    key_pos,
    kcum_small,
    kcum_large,
):
    key_count = key_pos.shape[0]
    block_width = math.gcd(key_count, 2048)
    blocks = key_count // block_width
    pieces = (
        part_small.reshape(blocks, block_width, part_small.shape[1]),
        part_large.reshape(blocks, block_width, part_large.shape[1]),
        key_pos.reshape(blocks, block_width),
        kcum_small.reshape(kcum_small.shape[0], blocks, block_width).transpose(1, 0, 2),
        kcum_large.reshape(kcum_large.shape[0], blocks, block_width).transpose(1, 0, 2),
    )
    query_last = query_pos[-1]

    def advance(carried, block_data):
        kv_one, kv_two, positions, cum_one, cum_two = block_data

        def compute(current):
            return (
                online_update(
                    current[0], query_small, qcum_small, kv_one, cum_one, positions, query_pos
                ),
                online_update(
                    current[1], query_large, qcum_large, kv_two, cum_two, positions, query_pos
                ),
            )

        return (
            lax.cond(jnp.min(positions) <= query_last, compute, lambda current: current, carried),
            None,
        )

    softmax_state, _ = lax.scan(advance, softmax_state, pieces)
    return softmax_state


def finish(carried):
    running_max, running_sum, weighted = carried
    outputs = (weighted / running_sum[:, :, None]).astype(jnp.bfloat16)
    return outputs.transpose(1, 0, 2).reshape(outputs.shape[1], outputs.shape[0] * outputs.shape[2])


def fresh_state(head_count, query_count, head_size):
    return (
        jnp.full((head_count, query_count), far_score, jnp.float32),
        jnp.zeros((head_count, query_count), jnp.float32),
        jnp.zeros((head_count, query_count, head_size), jnp.float32),
    )


def on_device(
    queries_small,
    queries_large,
    kv_small,
    kv_large,
    cum_small,
    cum_large,
    residual,
    out_small,
    out_large,
    gain_mix,
    gain_route,
    gain_blend,
    w_gate,
    w_up,
    w_down,
    route,
    route_bias,
):
    tokens_here = queries_small.shape[0]
    heads_small = cum_small.shape[0]
    heads_large = cum_large.shape[0]
    size_small = kv_small.shape[1] // 2
    size_large = kv_large.shape[1] // 2
    query_small = queries_small.reshape(tokens_here, heads_small, size_small)
    query_large = queries_large.reshape(tokens_here, heads_large, size_large)
    query_pos = lax.axis_index("sp") * tokens_here + jnp.arange(tokens_here, dtype=jnp.int32)
    cum_all = sent_together((cum_small, cum_large), "sp", 1, 0)
    start_state = (
        fresh_state(heads_small, tokens_here, size_small),
        fresh_state(heads_large, tokens_here, size_large),
    )
    block_data = sent_together_2((kv_small, kv_large), "sp", 0, 1)
    key_count = block_data[0].shape[0]
    key_pos = jnp.arange(key_count, dtype=jnp.int32)
    kcum_small = cum_all[0]
    kcum_large = cum_all[1]
    softmax_state = attend_keys(
        start_state,
        query_small,
        query_large,
        cum_small,
        cum_large,
        query_pos,
        block_data[0],
        block_data[1],
        key_pos,
        kcum_small,
        kcum_large,
    )
    attn_small = finish(softmax_state[0])
    attn_large = finish(softmax_state[1])
    row_count = tokens_here // lax.axis_size("tp")
    weight_small = lax.dynamic_slice_in_dim(
        out_small, lax.axis_index("tp") * attn_small.shape[1], attn_small.shape[1], 0
    )
    weight_large = lax.dynamic_slice_in_dim(
        out_large, lax.axis_index("tp") * attn_large.shape[1], attn_large.shape[1], 0
    )
    mixer_out = sum_at_owner(
        (
            jnp.dot(attn_small, weight_small, preferred_element_type=jnp.float32)
            + jnp.dot(attn_large, weight_large, preferred_element_type=jnp.float32)
        ).astype(jnp.bfloat16),
        "tp",
        0,
    )
    mixed = (residual.astype(jnp.float32) + rms_scale(mixer_out, gain_mix)).astype(jnp.bfloat16)
    routed = rms_scale(mixed.astype(jnp.float32), gain_route).astype(jnp.bfloat16)
    experts = lax.axis_size(("sp", "tp"))
    capacity = 4 * row_count // experts
    flat_ids = route.reshape(2 * row_count)
    marked = (flat_ids[:, None] == jnp.arange(experts, dtype=jnp.int32)[None, :]).astype(jnp.int32)
    ranked = jnp.sum((jnp.cumsum(marked, axis=0) - 1) * marked, axis=1)
    slot_ids = flat_ids * capacity + ranked
    dispatch_table = (
        slot_ids[:, None] == jnp.arange(experts * capacity, dtype=jnp.int32)[None, :]
    ).astype(jnp.bfloat16)
    dispatch_table = dispatch_table[:row_count] + dispatch_table[row_count:]
    outgoing = jnp.einsum(
        "rs,rd->sd", dispatch_table, routed, preferred_element_type=jnp.float32
    ).astype(jnp.bfloat16)
    outgoing = outgoing.reshape(experts, capacity, routed.shape[1])
    received = lax.all_to_all(outgoing, ("sp", "tp"), split_axis=0, concat_axis=0, tiled=True)
    row_total = received.shape[0] * received.shape[1]
    expert_rows = received.reshape(row_total, received.shape[2])
    gate_pre = jnp.dot(expert_rows, w_gate[0], preferred_element_type=jnp.float32)
    up_pre = jnp.dot(expert_rows, w_up[0], preferred_element_type=jnp.float32)
    hidden = (jax.nn.silu(gate_pre) * up_pre).astype(jnp.bfloat16)
    expert_out = jnp.dot(hidden, w_down[0], preferred_element_type=jnp.float32).astype(jnp.bfloat16)
    returned = lax.all_to_all(
        expert_out.reshape(received.shape), ("sp", "tp"), split_axis=0, concat_axis=0, tiled=True
    )
    picked = returned.reshape(experts * capacity, routed.shape[1])[slot_ids].astype(jnp.float32)
    blended = (
        jax.nn.sigmoid(route_bias)[:, None] * picked[:row_count]
        + jax.nn.sigmoid(-route_bias)[:, None] * picked[row_count:]
    )
    return (mixed.astype(jnp.float32) + rms_scale(blended, gain_blend)).astype(jnp.bfloat16)


def solution(mesh):
    in_specs = (
        P("sp", "tp"),
        P("sp", "tp"),
        P("sp", None),
        P("sp", None),
        P("tp", "sp"),
        P("tp", "sp"),
        P(("sp", "tp"), None),
        P(),
        P(),
        P(),
        P(),
        P(),
        P(("sp", "tp"), None, None),
        P(("sp", "tp"), None, None),
        P(("sp", "tp"), None, None),
        P(None, ("sp", "tp")),
        P(("sp", "tp")),
    )
    out_specs = P(("sp", "tp"), None)
    return jax.shard_map(
        on_device, mesh=mesh, in_specs=in_specs, out_specs=out_specs, check_vma=False
    )
```

profile of v0, /device:TPU:1, one launch (start us, length us, event | category | flops | bytes accessed | tf_op | source)
XLA Modules:
  0.0 490.0 jit_solution(5262072869251792836)
XLA Ops:
  6.5 1.6 pad_maximum_fusion
  8.1 0.0 all-gather.2.cloned.1.call-update
  8.2 0.7 pad_maximum_fusion.1
  8.9 1.2 broadcast_in_dim.105
  10.1 12.0 %all-to-all-start = ((f32[64,12,256]{2,1,0:T(8,128)}), f32[64,12,256]{2,1,0:T(8,128)S(1)}, u32[]{:S(2)}, u32[]{:S(2)}) async-start(f32[64,12,256]{2,1,0:T(8,128)} %broadcast_in_dim.105), calls=%async_computation | async-start | bytes 2097152 | tf_op jit(solution)/shard_map/all_to_all | solution.py:14
  22.0 0.6 slice.49
  22.7 1.1 copy.24
  23.7 1.1 copy.25
  24.8 0.2 copy.27
  25.0 0.8 copy.29
  25.8 0.2 fusion.58
  26.1 0.1 add_add_fusion
  26.2 0.9 fusion.60
  27.0 0.7 multiply_add_fusion.3
  27.7 0.8 fusion.57
  28.5 12.8 %all-to-all-done = f32[64,12,256]{2,1,0:T(8,128)S(1)} async-done(((f32[64,12,256]{2,1,0:T(8,128)}), f32[64,12,256]{2,1,0:T(8,128)S(1)}, u32[]{:S(2)}, u32[]{:S(2)}) %all-to-all-start) | async-done | bytes 786464 | tf_op jit(solution)/shard_map/all_to_all | solution.py:14
  41.4 68.5 %all-gather.2.cloned.1.call-done = bf16[16384,384]{1,0:T(8,128)(2,1)} async-done(((bf16[256,384]{1,0:T(8,128)(2,1)}), bf16[16384,384]{1,0:T(8,128)(2,1)}) %all-gather.2.cloned.1.call-update) | async-done | bytes 12582928 | tf_op jit(solution)/shard_map/all_gather | solution.py:42
  109.9 3.7 split.8
  113.5 6.5 %copy.26 = bf16[8,2048,128]{1,2,0:T(8,128)(2,1)} copy(bf16[8,2048,128]{2,1,0:T(8,128)(2,1)} %bitcast.109) | data formatting | bytes 8388608
  120.1 7.0 %split.9 = bf16[16384,256]{1,0:T(8,128)(2,1)} slice(bf16[16384,384]{1,0:T(8,128)(2,1)} %all-gather.2.cloned.1.call-done), slice={[0:16384], [128:384]} | slice | bytes 16777216 | tf_op jit(solution)/shard_map/split | solution.py:43
  127.2 43.4 %while.21 = (s32[]{:T(128)}, f32[8,256]{1,0:T(8,128)S(1)}, f32[8,256]{1,0:T(8,128)S(1)}, f32[8,256,64]{1,2,0:T(8,128)S(1)}, f32[4,256]{1,0:T(4,128)S(1)}, /*inde...) while((s32[]{:T(128)}, f32[8,256]{1,0:T(8,128)S(1)}, ...), condition=%wide.region_8.9_spmd.clone, body=%wide.region_0.8_spmd.clone.sunk | while | flops 2268078336 | bytes 87261648 | solution.py:128
  127.4 0.6 fusion.74
  129.3 27.8 %conditional.3 = ((f32[8,256]{1,0:T(8,128)S(1)}, f32[8,256]{1,0:T(8,128)S(1)}, f32[8,256,64]{1,2,0:T(8,128)S(1)}, f32[4,256]{1,0:T(4,128)S(1)}, f32[4,256]{1,0:T(4,128)S(1)}, /*index=5*/f32[4,256,128]{2,1,0:T(8,128)S(1)})) conditional(s32[]{:T(128)} %convert_element_type.117, (f32[8,256]{1,0:T(8,128)S(1)}, f32[8,256]{1,0:T(8,128)S(1)}, ...), branch_computations={%region_2.2_spmd, %region_3.7_spmd} | conditional | flops 2268076288 | bytes 87243848 | solution.py:124
  129.4 0.5 broadcast_compare_fusion
  129.8 1.1 dynamic-slice_bitcast_fusion.1
  130.9 4.4 fusion.6
  135.3 6.0 %fusion.5 = f32[8,256]{1,0:T(8,128)S(1)} fusion(f32[2048,256,8]{1,0,2:T(8,128)S(1)} %get-tuple-element.376, f32[8,256]{1,0:T(8,128)S(1)} %max.8, f32[8,2048]{1,0:T(8,128)S(1)} %dynamic-slice_bitcast_fusion.2, f32[8,256]{1,0:T(8,128)S(1)} %get-tuple-element.221, pred[256,2048]{0,1:T(8,128)(4,1)S(1)} %broadcast_compare_fusion), kind=kLoop, calls=%fused_computation.7 | loop fusion | flops 29358080 | bytes 17391616 | tf_op jit(solution)/shard_map/while/body/eval_jaxpr/cond/branch_1_fun/reduce_sum | solution.py:78
  141.4 5.6 %fusion.21 = f32[8,256,64]{1,2,0:T(8,128)S(1)} fusion(f32[2048,256,8]{1,0,2:T(8,128)S(1)} %get-tuple-element.376, f32[8,256]{1,0:T(8,128)S(1)} %max.8, f32[8,2048]{1,0:T(8,128)S(1)} %dynamic-slice_bitcast_fusion.2, f32[8,256]{1,0:T(8,128)S(1)} %get-tuple-element.221, pred[256,2048]{0,1:T(8,128)(4,1)S(1)} %broadcast_compare_fusion, ...), kind=kOutput, calls=%fused_computation.21 | convolution fusion | flops 566493184 | bytes 18702336 | tf_op jit(solution)/shard_map/while/body/eval_jaxpr/cond/branch_1_fun/hqk,kd->hqd/dot_general | solution.py:79
  147.0 1.3 dynamic-slice_bitcast_fusion
  148.3 2.2 fusion.14
  150.5 2.9 fusion.13
  153.4 3.7 fusion.18
  157.1 0.6 fusion.74
  159.0 0.6 fusion.74
  160.9 0.6 fusion.74
  162.8 0.6 fusion.74
  164.7 0.6 fusion.74
  166.6 0.6 fusion.74
  168.5 0.6 fusion.74
  170.6 0.2 copy.28
  170.8 0.0 copy-start.2
  170.9 0.0 copy-start.8
  171.0 0.0 copy-start.1
  171.0 2.4 fusion.43
  173.4 2.3 fusion.41
  175.7 5.0 %all_to_all.20 = bf16[2,128,2048]{2,1,0:T(8,128)(2,1)S(1)} all-to-all(bf16[2,128,2048]{2,1,0:T(8,128)(2,1)S(1)} %bitcast.110), channel_id=1, replica_groups=mesh['sp'=64,'tp'=2] {'tp'}, dimensions={0} | all-to-all | bytes 2097152 | tf_op jit(solution)/shard_map/all_to_all | solution.py:54
  180.7 0.2 convert_reduce_fusion
  180.9 0.2 multiply_reduce_fusion.1
  181.1 0.4 fusion.47
  181.5 0.8 convolution_convert_fusion
  182.3 2.2 reshape.197
  184.6 232.2 %all_to_all.21 = bf16[128,4,2048]{2,1,0:T(4,128)(2,1)S(1)} all-to-all(bf16[128,4,2048]{2,1,0:T(4,128)(2,1)} %reshape.197), channel_id=1, replica_groups=mesh['sp'=64,'tp'=2] {'sp','tp'}, dimensions={0} | all-to-all | bytes 4194304 | tf_op jit(solution)/shard_map/all_to_all | solution.py:229
  416.8 2.0 reshape.198
  418.8 6.6 %fusion.36 = f32[512,1024]{1,0:T(8,128)} fusion(bf16[512,2048]{1,0:T(8,128)(2,1)} %reshape.198, bf16[1,2048,1024]{2,1,0:T(8,128)(2,1)} %param.33), kind=kOutput, calls=%fused_computation.49 | convolution fusion | flops 2147483648 | bytes 8388608 | tf_op jit(solution)/shard_map/dot_general | solution.py:232
  425.5 9.9 %fusion.38 = bf16[512,2048]{1,0:T(8,128)(2,1)} fusion(bf16[1,1024,2048]{2,1,0:T(8,128)(2,1)} %param.35, f32[512,1024]{1,0:T(8,128)} %fusion.36, bf16[512,2048]{1,0:T(8,128)(2,1)S(1)} %copy-done, bf16[1,2048,1024]{2,1,0:T(8,128)(2,1)} %param.34), kind=kOutput, calls=%fused_computation.51 | convolution fusion | flops 4299161600 | bytes 14680064 | tf_op jit(solution)/shard_map/dot_general | solution.py:235
  435.4 4.1 reshape.199
  439.5 5.5 %all-to-all-start.3 = ((bf16[128,4,2048]{2,1,0:T(4,128)(2,1)}), bf16[128,4,2048]{2,1,0:T(4,128)(2,1)}, u32[]{:S(2)}, u32[]{:S(2)}) async-start(bf16[128,4,2048]{2,1,0:T(4,128)(2,1)} %reshape.199), calls=%async_computation.3 | async-start | bytes 4194304 | tf_op jit(solution)/shard_map/all_to_all | solution.py:236
  445.1 30.2 %all-to-all-done.3 = bf16[128,4,2048]{2,1,0:T(4,128)(2,1)} async-done(((bf16[128,4,2048]{2,1,0:T(4,128)(2,1)}), bf16[128,4,2048]{2,1,0:T(4,128)(2,1)}, u32[]{:S(2)}, u32[]{:S(2)}) %all-to-all-start.3) | async-done | bytes 2097184 | tf_op jit(solution)/shard_map/all_to_all | solution.py:236
  475.2 2.5 reshape.200
  477.8 0.0 copy-start.10
  477.8 2.3 gather_fusion
  480.1 1.5 convert_element_type.74
  481.6 0.3 multiply_reduce_fusion
  481.9 1.2 fusion.50
  (68 shorter events, 0.6 us)
Async XLA Ops:
  6.5 103.3 %all-gather.2.cloned.1.call-start = ((), (), s32[]{:S(2)}) async-start(), calls=%async_computation.4 | async-start | bytes 12779520 | tf_op jit(solution)/shard_map/all_gather | solution.py:42
  10.1 31.2 %all-to-all-start = ((f32[64,12,256]{2,1,0:T(8,128)}), f32[64,12,256]{2,1,0:T(8,128)S(1)}, u32[]{:S(2)}, u32[]{:S(2)}) async-start(f32[64,12,256]{2,1,0:T(8,128)} %broadcast_in_dim.105), calls=%async_computation | async-start | bytes 2097152 | tf_op jit(solution)/shard_map/all_to_all | solution.py:14
  27.0 14.3 %copy-start.6 = (s32[256]{0:T(256)}, s32[256]{0:T(256)S(1)}, u32[]{:S(2)}) copy-start(s32[256]{0:T(256)S(1)} %fusion.60) | copy-start | bytes 3076
  120.1 7.2 %copy-start.3 = (f32[8,256]{1,0:T(8,128)S(1)}, f32[8,256]{1,0:T(8,128)}, u32[]{:S(2)}) copy-start(f32[8,256]{1,0:T(8,128)} %param.25) | copy-start | bytes 24580
  120.1 7.2 %copy-start.4 = (f32[4,256]{1,0:T(4,128)S(1)}, f32[4,256]{1,0:T(4,128)}, u32[]{:S(2)}) copy-start(f32[4,256]{1,0:T(4,128)} %param.26) | copy-start | bytes 12292
  170.8 10.3 %copy-start.2 = (bf16[128,2048]{1,0:T(8,128)(2,1)S(1)}, bf16[128,2048]{1,0:T(8,128)(2,1)}, u32[]{:S(2)}) copy-start(bf16[128,2048]{1,0:T(8,128)(2,1)} %param.27) | copy-start | bytes 1572868
  170.9 10.3 %copy-start.8 = (f32[2048]{0:T(1024)S(1)}, f32[2048]{0:T(1024)}, u32[]{:S(2)}) copy-start(f32[2048]{0:T(1024)} %param.30) | copy-start | bytes 24580
  171.0 10.5 %copy-start.1 = (bf16[256,512]{1,0:T(8,128)(2,1)S(1)}, bf16[256,512]{1,0:T(8,128)(2,1)}, u32[]{:S(2)}) copy-start(bf16[256,512]{1,0:T(8,128)(2,1)} %fusion.57) | copy-start | bytes 786436
  171.0 10.5 %copy-start.9 = (f32[2048]{0:T(1024)S(1)}, f32[2048]{0:T(1024)}, u32[]{:S(2)}) copy-start(f32[2048]{0:T(1024)} %param.31) | copy-start | bytes 24580
  418.8 6.7 %copy-start = (bf16[512,2048]{1,0:T(8,128)(2,1)S(1)}, bf16[512,2048]{1,0:T(8,128)(2,1)}, u32[]{:S(2)}) copy-start(bf16[512,2048]{1,0:T(8,128)(2,1)} %reshape.198) | copy-start | bytes 6291460
  435.4 9.6 %copy-start.5 = (s32[2,128]{1,0:T(2,128)S(1)}, s32[2,128]{1,0:T(2,128)}, u32[]{:S(2)}) copy-start(s32[2,128]{1,0:T(2,128)} %param.36) | copy-start | bytes 3076
  435.4 9.6 %copy-start.7 = (s32[256]{0:T(256)S(1)}, s32[256]{0:T(256)}, u32[]{:S(2)}) copy-start(s32[256]{0:T(256)} %copy-done.6) | copy-start | bytes 3076
  435.4 9.7 %copy-start.11 = (f32[128]{0:T(128)S(1)}, f32[128]{0:T(128)}, u32[]{:S(2)}) copy-start(f32[128]{0:T(128)} %param.37) | copy-start | bytes 1540
  439.5 35.7 %all-to-all-start.3 = ((bf16[128,4,2048]{2,1,0:T(4,128)(2,1)}), bf16[128,4,2048]{2,1,0:T(4,128)(2,1)}, u32[]{:S(2)}, u32[]{:S(2)}) async-start(bf16[128,4,2048]{2,1,0:T(4,128)(2,1)} %reshape.199), calls=%async_computation.3 | async-start | bytes 4194304 | tf_op jit(solution)/shard_map/all_to_all | solution.py:236
  477.8 4.2 copy-start.10
Sparse Core Ops, SparseCore 0:
  10.1 99.7 all-gather.1
where the time goes:
time: 492 us; the launch traced here: 490 us
  blocking collectives  237 us (48%)
  waiting for transfers between devices  111 us (23%)
  local copies, waits for them, and re-layouts  38.3 us (8%)
  matrix products  37.9 us (8%)
  other arithmetic  23.4 us (5%)
  starting transfers between devices  17.4 us (4%)
  between operations  13.8 us (3%)
  loops' own time  10.5 us (2%)
    all_to_all x1, blocking collectives, on_device(): lax.all_to_all(outgoing, ('sp', 'tp'), split_axis=0, concat_axis=0, tiled...  232 us
    all_gather x1, waiting for transfers between devices, sent_together_2(): out = lax.all_gather(both, axis, axis=dim, tiled=True)  68.5 us
    all_to_all x1, waiting for transfers between devices, on_device(): lax.all_to_all(expert_out.reshape(received.shape), ('sp', 'tp'), split_ax...  30.2 us
    all_to_all x1, waiting for transfers between devices, sent_to_all(): lax.all_to_all(jnp.broadcast_to(array[None], (devices, *array.shape)), ax...  12.8 us
    all_to_all x1, starting transfers between devices, sent_to_all(): lax.all_to_all(jnp.broadcast_to(array[None], (devices, *array.shape)), ax...  12 us
    split x2, local copies, waits for them, and re-layouts, sent_together_2(): jnp.split(out, [sum(widths[:k]) for k in range(1, len(widths))], axis=along)  10.7 us
    another operation x1, loops' own time, attend_keys(): softmax_state, _ = lax.scan(advance, softmax_state, pieces)  10.3 us
    dot_general x1, matrix products, on_device(): jnp.dot(hidden, w_down[0], preferred_element_type=jnp.float32)  9.9 us
  transfers between devices with their start and end apart: 3, of which 3 were waited for; matrix products, arithmetic and copies ran while one was open for 2% of the time, Pallas kernels for 0%

commit v1 on v0

v1 whole, which is shorter than its diff:
```python
import functools
import math

import jax
import jax.numpy as jnp
from jax import lax
from jax.experimental import pallas as pl
from jax.experimental.pallas import tpu as pltpu
from jax.sharding import PartitionSpec as P

MESH = pl.DeviceIdType.MESH
norm_eps = 1e-06
far_score = -1e30
log2e = 1.4426950408889634
f32, bf16 = jnp.float32, jnp.bfloat16
unit = 1024
own_units = 9

orders = (("x", "y", "z"), ("y", "z", "x"), ("z", "x", "y"))
pieces = (
    (0, 0, 0, 32, 16),
    (1, 0, 48, 32, 16),
    (2, 0, 96, 32, 16),
    (0, 0, 32, 16, 8),
    (1, 0, 80, 16, 8),
    (2, 1, 0, 24, 16),
)
shift = (3, 1, 2, 2)

def gather_kernel(kv_ref, cum_ref, g_ref, c_ref, local, send, recv, dsend, drecv):
    sp, tp = lax.axis_index("sp"), lax.axis_index("tp")
    at = {"z": sp // 16, "y": (sp // 4) % 4, "x": sp % 4}
    partner = (sp, 1 - tp)

    def moved(dim, by):
        here = dict(at)
        here[dim] = (at[dim] + by) % 4
        return (here["z"] * 16 + here["y"] * 4 + here["x"], tp)

    barrier = pltpu.get_barrier_semaphore()
    for dim in ("x", "y", "z"):
        for by in (1, 3):
            pl.semaphore_signal(barrier, inc=1, device_id=moved(dim, by), device_id_type=MESH)
    pl.semaphore_signal(barrier, inc=1, device_id=partner, device_id_type=MESH)

    def rows_of(piece, kind):
        _, _, first, count, half = pieces[piece]
        if kind == 2:
            return (first, half)
        if kind == 3:
            return (first + half, count - half)
        return (first, count)

    def view(piece, phase, offset, kind, side):
        order = orders[pieces[piece][0]]
        index = []
        for dim in ("z", "y", "x"):
            where = order.index(dim)
            if where < phase:
                index.append(slice(None))
            else:
                index.append((at[dim] + offset) % 4 if where == phase else at[dim])
        whole = c_ref if pieces[piece][1] else g_ref
        return whole.at[(*index, side, pl.ds(*rows_of(piece, kind)), slice(None))]

    def sent(piece, phase, kind):
        target = view(piece, phase, (0, 0, 3, 1)[kind], kind, tp)
        source = target
        if phase == 0 and kind < 2:
            source = (cum_ref if pieces[piece][1] else kv_ref).at[pl.ds(*rows_of(piece, kind)), :]
        return pltpu.make_async_remote_copy(
            src_ref=source, dst_ref=target, send_sem=send.at[piece, phase, kind], recv_sem=recv.at[piece, phase, kind],
            device_id=moved(orders[pieces[piece][0]][phase], 1 if kind in (0, 2) else 3), device_id_type=MESH)

    def arrived(piece, phase, kind):
        ref = view(piece, phase, shift[kind], kind, tp)
        return pltpu.make_async_remote_copy(
            src_ref=ref, dst_ref=ref, send_sem=send.at[piece, phase, kind], recv_sem=recv.at[piece, phase, kind],
            device_id=partner, device_id_type=MESH)

    def shared(piece, phase, kind, side):
        ref = view(piece, phase, shift[kind], kind, side)
        return pltpu.make_async_remote_copy(
            src_ref=ref, dst_ref=ref, send_sem=dsend.at[piece, phase, kind], recv_sem=drecv.at[piece, phase, kind],
            device_id=partner, device_id_type=MESH)

    def own(source, whole, k):
        return pltpu.make_async_remote_copy(
            src_ref=source, dst_ref=whole.at[at["z"], at["y"], at["x"], tp], send_sem=local.at[2 + k], recv_sem=local.at[4 + k],
            device_id=partner, device_id_type=MESH)

    def kept(source, whole, k):
        return pltpu.make_async_copy(source, whole.at[at["z"], at["y"], at["x"], tp], local.at[k])

    count = range(len(pieces))
    kept(kv_ref, g_ref, 0).start()
    kept(cum_ref, c_ref, 1).start()
    pl.semaphore_wait(barrier, 7)
    for piece in count:
        for kind in (0, 1):
            sent(piece, 0, kind).start()
    own(kv_ref, g_ref, 0).start()
    own(cum_ref, c_ref, 1).start()
    kept(kv_ref, g_ref, 0).wait()
    kept(cum_ref, c_ref, 1).wait()
    for phase in range(3):
        for piece in count:
            for kind in (0, 1):
                arrived(piece, phase, kind).wait_recv()
                sent(piece, phase, 2 + kind).start()
                shared(piece, phase, kind, tp).start()
        for piece in count:
            for kind in (2, 3):
                arrived(piece, phase, kind).wait_recv()
            if phase < 2:
                for kind in (0, 1):
                    sent(piece, phase + 1, kind).start()
            for kind in (2, 3):
                shared(piece, phase, kind, tp).start()
    for k, whole in ((0, g_ref), (1, c_ref)):
        source = kv_ref if k == 0 else cum_ref
        own(source, whole, k).wait_send()
        theirs = whole.at[at["z"], at["y"], at["x"], 1 - tp]
        pltpu.make_async_remote_copy(
            src_ref=theirs, dst_ref=theirs, send_sem=local.at[2 + k], recv_sem=local.at[4 + k],
            device_id=partner, device_id_type=MESH).wait_recv()
    for phase in range(3):
        for piece in count:
            for kind in range(4):
                sent(piece, phase, kind).wait_send()
                shared(piece, phase, kind, tp).wait_send()
                shared(piece, phase, kind, 1 - tp).wait_recv()

def gather(kv, cum):
    DMA = pltpu.SemaphoreType.DMA
    shape = (len(pieces), 3, 4)
    V = pl.BlockSpec(memory_space=pltpu.VMEM)
    O = pl.BlockSpec(memory_space=pl.ANY)
    return pl.pallas_call(
        gather_kernel,
        out_shape=(jax.ShapeDtypeStruct((4, 4, 4, 2, 128, 384), jnp.bfloat16), jax.ShapeDtypeStruct((4, 4, 4, 2, 24, 128), jnp.float32)),
        in_specs=[V, V],
        out_specs=(O, O),
        scratch_shapes=[DMA((6,)), DMA(shape), DMA(shape), DMA(shape), DMA(shape)],
        compiler_params=pltpu.CompilerParams(collective_id=0, has_side_effects=True, vmem_limit_bytes=40*1024*1024),
        name="gather_keys",
    )(kv, cum)


def attention_kernel(bounds, qs_ref, ql_ref, cq_ref, g_ref, c_ref, os_ref, ol_ref, ml_ref,
                     kv, gates, tile, vts, vtl, qs, ql, acc_s, acc_l, top, sems, *, diagonal):
    lo, hi, q0, first_head = bounds[0], bounds[1], bounds[2], bounds[3]
    nq = 256
    cs, cl = log2e / 8.0, log2e / math.sqrt(128.0)
    n = hi - lo

    def fetch(u, slot):
        return (
            pltpu.make_async_copy(g_ref.at[pl.ds(pl.multiple_of(u * unit, unit), unit), :], kv.at[slot], sems.at[0, slot]),
            pltpu.make_async_copy(c_ref.at[pl.ds(u * 8, 8)], gates.at[slot], sems.at[1, slot]),
        )

    @pl.when(n > 0)
    def _():
        for copy in fetch(hi - 1, 0):
            copy.start()

    acc_s[...] = jnp.zeros(acc_s.shape, f32)
    acc_l[...] = jnp.zeros(acc_l.shape, f32)
    top[...] = jnp.zeros(top.shape, f32)
    vts[64:80, :] = jnp.ones((16, unit), bf16)
    vtl[128:144, :] = jnp.ones((16, unit), bf16)
    qs[128:192, :] = qs_ref[...]
    qs[192:256, :] = jnp.zeros((64, 2048), bf16)
    ql[0:128, :] = ql_ref[...]
    row = lax.broadcasted_iota(jnp.int32, (128, nq), 0)
    for h in range(12):
        head = first_head + h
        here = cq_ref[h : h + 1, :]
        high = here.astype(bf16).astype(f32)
        rest = here - high
        middle = rest.astype(bf16).astype(f32)
        low = rest - middle
        chosen = jnp.where((row == head) | (row == 24 + head) | (row == 48 + head), -8.0, 0.0)
        chosen = jnp.where(row == 72, 8.0 * high, chosen)
        chosen = jnp.where(row == 73, 8.0 * middle, chosen)
        chosen = jnp.where(row == 74, 8.0 * low, chosen).astype(bf16)
        if h < 8:
            qs[0:128, h * nq : (h + 1) * nq] = chosen
        else:
            ql[128:256, (h - 8) * nq : (h - 7) * nq] = chosen
    size_s = jnp.max(jnp.sum(jnp.abs(qs_ref[...].astype(f32)), axis=0, keepdims=True))
    size_l = jnp.max(jnp.sum(jnp.abs(ql_ref[...].astype(f32)), axis=0, keepdims=True))
    bounded = (size_s <= 150.0) & (size_l <= 210.0)

    def ready(i):
        u, slot = hi - 1 - i, lax.rem(i, 2)
        for copy in fetch(u, slot):
            copy.wait()

        @pl.when(i + 1 < n)
        def _():
            for copy in fetch(u - 1, 1 - slot):
                copy.start()

        for j in range(8):
            gate = gates[slot, j]
            high = gate.astype(bf16).astype(f32)
            rest = gate - high
            middle = rest.astype(bf16).astype(f32)
            wide = jnp.concatenate([high, middle, rest - middle, jnp.ones((8, 128), f32), jnp.zeros((48, 128), f32)], axis=0)
            tile[j * 128 : (j + 1) * 128, :] = wide.T.astype(bf16)
        vts[0:64, :] = kv[slot, :, 0:128].T[64:128, :]
        vtl[0:128, :] = kv[slot, :, 256:384].T
        return u, slot

    def keys_small(slot):
        return jnp.concatenate([tile[...], kv[slot, :, 0:128]], axis=1)

    def keys_large(slot):
        return jnp.concatenate([kv[slot, :, 128:256], tile[...]], axis=1)

    def allowed(u, width):
        key = u * unit + lax.broadcasted_iota(jnp.int32, (unit, width), 0)
        query = q0 + (lax.broadcasted_iota(jnp.int32, (unit, width), 1) & (nq - 1))
        return key <= query

    def quick(i, masked):
        u, slot = ready(i)
        for keys, q, w, vt, acc, scale in (
            (keys_small, qs, 0, vts, acc_s, cs),
            (keys_small, qs, 1024, vts, acc_s, cs),
            (keys_large, ql, 0, vtl, acc_l, cl),
        ):
            s = jnp.dot(keys(slot), q[:, w : w + 1024], preferred_element_type=f32) * scale
            if masked:
                s = jnp.where(allowed(u, 1024), s, far_score)
            p = jnp.exp2(s).astype(bf16)
            acc[:, w : w + 1024] += jnp.dot(vt[...], p, preferred_element_type=f32)

    def careful(i, _):
        u, slot = ready(i)

        def group(keys, q, vt, acc, scale, count, base):
            def head(h, _):
                w = pl.ds(pl.multiple_of(h * nq, nq), nq)
                s = jnp.dot(keys(slot), q[:, w], preferred_element_type=f32) * scale
                s = jnp.where(allowed(u, nq), s, far_score)
                before = top[base + h]
                after = jnp.maximum(before, jnp.max(s, axis=0, keepdims=True))
                top[base + h] = after
                p = jnp.exp2(s - after).astype(bf16)
                acc[:, w] = acc[:, w] * jnp.exp2(before - after) + jnp.dot(vt[...], p, preferred_element_type=f32)
                return 0

            lax.fori_loop(0, count, head, 0)

        group(keys_small, qs, vts, acc_s, cs, 8, 0)
        group(keys_large, ql, vtl, acc_l, cl, 4, 8)
        return 0

    @pl.when(bounded)
    def _():
        if diagonal:
            quick(0, True)
        lax.fori_loop(1 if diagonal else 0, n, lambda i, _: (quick(i, False), 0)[1], 0)

    @pl.when(jnp.logical_not(bounded))
    def _():
        top[...] = jnp.full(top.shape, far_score, f32)
        lax.fori_loop(0, n, careful, 0)

    ml_ref[...] = jnp.zeros(ml_ref.shape, f32)
    for h in range(12):
        size, acc, out, k = (64, acc_s, os_ref, h) if h < 8 else (128, acc_l, ol_ref, h - 8)
        w = slice(k * nq, (k + 1) * nq)
        total = acc[size : size + 1, w]
        scale = jnp.where(total > 0, 1.0 / jnp.where(total > 0, total, 1.0), 0.0)
        out[k * size : (k + 1) * size, :] = (acc[0:size, w] * scale).astype(out.dtype)
        ml_ref[h : h + 1, :] = top[h]
        ml_ref[16 + h : 17 + h, :] = total


def attention(bounds, qs, ql, cq, g, c, diagonal):
    V = pl.BlockSpec(memory_space=pltpu.VMEM)
    A = pl.BlockSpec(memory_space=pl.ANY)
    kind = f32 if diagonal else bf16
    VM = pltpu.VMEM
    return pl.pallas_call(
        functools.partial(attention_kernel, diagonal=diagonal),
        out_shape=(
            jax.ShapeDtypeStruct((512, 256), kind),
            jax.ShapeDtypeStruct((512, 256), kind),
            jax.ShapeDtypeStruct((32, 256), f32),
        ),
        in_specs=[pl.BlockSpec(memory_space=pltpu.SMEM), V, V, V, A, A],
        out_specs=(V, V, V),
        scratch_shapes=[
            VM((2, unit, 384), bf16), VM((2, 8, 24, 128), f32), VM((unit, 128), bf16),
            VM((80, unit), bf16), VM((144, unit), bf16), VM((256, 2048), bf16), VM((256, 1024), bf16),
            VM((80, 2048), f32), VM((144, 1024), f32), VM((12, 1, 256), f32), pltpu.SemaphoreType.DMA((2, 2)),
        ],
        compiler_params=pltpu.CompilerParams(vmem_limit_bytes=50 * 1024 * 1024),
        cost_estimate=pl.CostEstimate(flops=12_000_000_000 if diagonal else 8_000_000_000, bytes_accessed=12_000_000, transcendentals=26_000_000),
        name="attention_own" if diagonal else "attention_far",
    )(bounds, qs, ql, cq, g, c)


def merged(own, far, m_own, m_far, l_own, l_far, heads):
    m_far = jnp.where(l_far > 0, m_far, far_score)
    most = jnp.maximum(m_own, m_far)
    a, b = l_own * jnp.exp2(m_own - most), l_far * jnp.exp2(m_far - most)
    whole = a + b
    size = own.shape[0] // heads
    own = own.reshape(heads, size, 256) * (a / whole)[:, None, :]
    far = far.astype(f32).reshape(heads, size, 256) * (b / whole)[:, None, :]
    return (own + far).astype(bf16).reshape(heads * size, 256)


def cut_along(array, dim, devices):
    lengths = array.shape
    tiles = array.reshape(*lengths[:dim], devices, lengths[dim] // devices, *lengths[dim + 1 :])
    return jnp.moveaxis(tiles, dim, 0)


def sum_at_owner(array, axis, dim):
    devices = lax.axis_size(axis)
    tiles = lax.all_to_all(cut_along(array, dim, devices), axis, 0, 0, tiled=True)
    return jnp.sum(tiles.astype(jnp.float32), axis=0)


def rms_scale(values, gain_row):
    return (
        values * lax.rsqrt(jnp.mean(values * values, axis=-1, keepdims=True) + norm_eps) * gain_row
    )


def on_device(
    queries_small,
    queries_large,
    kv_small,
    kv_large,
    cum_small,
    cum_large,
    residual,
    out_small,
    out_large,
    gain_mix,
    gain_route,
    gain_blend,
    w_gate,
    w_up,
    w_down,
    route,
    route_bias,
):
    sp, tp = lax.axis_index("sp"), lax.axis_index("tp")
    tokens_here = queries_small.shape[0]
    chips = lax.axis_size("sp")
    gates = jnp.concatenate([cum_small, cum_large * jnp.float32(math.sqrt(2.0))], axis=0)
    halves = gates.reshape(12, 2, 128)
    kept = lax.dynamic_index_in_dim(halves, tp, 1, keepdims=False)
    given = lax.ppermute(lax.dynamic_index_in_dim(halves, 1 - tp, 1, keepdims=False), "tp", [(0, 1), (1, 0)])
    all_gates = jnp.where(tp == 0, jnp.concatenate([kept, given], axis=0), jnp.concatenate([given, kept], axis=0))
    kv_here = jnp.concatenate(
        [lax.dynamic_slice_in_dim(kv, tp * 128, 128, 0) for kv in (kv_small, kv_large)], axis=1
    )
    qs = queries_small.reshape(256, 8, 64).transpose(2, 1, 0).reshape(64, 2048)
    ql = queries_large.reshape(256, 4, 128).transpose(2, 1, 0).reshape(128, 1024)
    cq = jnp.concatenate([gates, jnp.zeros((4, 256), f32)], axis=0)
    to_early = [(chips - 1 - i, i) for i in range(chips // 2)]
    to_late = [(i, chips - 1 - i) for i in range(chips // 2)]
    far_q = [lax.ppermute(a, "sp", to_early) for a in (qs, ql, cq)]
    g, c = gather(kv_here, all_gates)
    g, c = g.reshape(chips * 256, 384), c.reshape(chips * 2, 24, 128)
    units = sp // 4 + 1
    first = jnp.maximum(units - own_units, 0)
    late = chips - 1 - sp
    helped = jnp.where(sp < chips // 2, jnp.maximum(late // 4 + 1 - own_units, 0), 0)
    bounds = jnp.stack([first, units, sp * 256, tp * 12]).astype(jnp.int32)
    far_bounds = jnp.stack([jnp.zeros_like(helped), helped, late * 256, tp * 12]).astype(jnp.int32)
    own_s, own_l, own_ml = attention(bounds, qs, ql, cq, g, c, True)
    far = attention(far_bounds, *far_q, g, c, False)
    far_s, far_l, far_ml = [lax.ppermute(a, "sp", to_late) for a in far]
    attn_small = merged(own_s, far_s, own_ml[0:8], far_ml[0:8], own_ml[16:24], far_ml[16:24], 8)
    attn_large = merged(own_l, far_l, own_ml[8:12], far_ml[8:12], own_ml[24:28], far_ml[24:28], 4)
    row_count = tokens_here // lax.axis_size("tp")
    weight_small = lax.dynamic_slice_in_dim(
        out_small, tp * 512, 512, 0
    )
    weight_large = lax.dynamic_slice_in_dim(
        out_large, tp * 512, 512, 0
    )
    mixer_out = sum_at_owner(
        (
            lax.dot_general(attn_small, weight_small, (((0,), (0,)), ((), ())), preferred_element_type=f32)
            + lax.dot_general(attn_large, weight_large, (((0,), (0,)), ((), ())), preferred_element_type=f32)
        ).astype(jnp.bfloat16),
        "tp",
        0,
    )
    mixed = (residual.astype(jnp.float32) + rms_scale(mixer_out, gain_mix)).astype(jnp.bfloat16)
    routed = rms_scale(mixed.astype(jnp.float32), gain_route).astype(jnp.bfloat16)
    experts = lax.axis_size(("sp", "tp"))
    capacity = 4 * row_count // experts
    flat_ids = route.reshape(2 * row_count)
    marked = (flat_ids[:, None] == jnp.arange(experts, dtype=jnp.int32)[None, :]).astype(jnp.int32)
    ranked = jnp.sum((jnp.cumsum(marked, axis=0) - 1) * marked, axis=1)
    slot_ids = flat_ids * capacity + ranked
    dispatch_table = (
        slot_ids[:, None] == jnp.arange(experts * capacity, dtype=jnp.int32)[None, :]
    ).astype(jnp.bfloat16)
    dispatch_table = dispatch_table[:row_count] + dispatch_table[row_count:]
    outgoing = jnp.einsum(
        "rs,rd->sd", dispatch_table, routed, preferred_element_type=jnp.float32
    ).astype(jnp.bfloat16)
    outgoing = outgoing.reshape(experts, capacity, routed.shape[1])
    received = lax.all_to_all(outgoing, ("sp", "tp"), split_axis=0, concat_axis=0, tiled=True)
    row_total = received.shape[0] * received.shape[1]
    expert_rows = received.reshape(row_total, received.shape[2])
    gate_pre = jnp.dot(expert_rows, w_gate[0], preferred_element_type=jnp.float32)
    up_pre = jnp.dot(expert_rows, w_up[0], preferred_element_type=jnp.float32)
    hidden = (jax.nn.silu(gate_pre) * up_pre).astype(jnp.bfloat16)
    expert_out = jnp.dot(hidden, w_down[0], preferred_element_type=jnp.float32).astype(jnp.bfloat16)
    returned = lax.all_to_all(
        expert_out.reshape(received.shape), ("sp", "tp"), split_axis=0, concat_axis=0, tiled=True
    )
    picked = returned.reshape(experts * capacity, routed.shape[1])[slot_ids].astype(jnp.float32)
    blended = (
        jax.nn.sigmoid(route_bias)[:, None] * picked[:row_count]
        + jax.nn.sigmoid(-route_bias)[:, None] * picked[row_count:]
    )
    return (mixed.astype(jnp.float32) + rms_scale(blended, gain_blend)).astype(jnp.bfloat16)


def solution(mesh):
    in_specs = (
        P("sp", "tp"),
        P("sp", "tp"),
        P("sp", None),
        P("sp", None),
        P("tp", "sp"),
        P("tp", "sp"),
        P(("sp", "tp"), None),
        P(),
        P(),
        P(),
        P(),
        P(),
        P(("sp", "tp"), None, None),
        P(("sp", "tp"), None, None),
        P(("sp", "tp"), None, None),
        P(None, ("sp", "tp")),
        P(("sp", "tp")),
    )
    out_specs = P(("sp", "tp"), None)
    return jax.shard_map(
        on_device, mesh=mesh, in_specs=in_specs, out_specs=out_specs, check_vma=False
    )
```

time: 492 us -> 290 us (0.59)
  blocking collectives: 237 us -> 94.6 us
  Pallas kernels: 0 us -> 82.5 us
  waiting for transfers between devices: 111 us -> 39.9 us
  matrix products: 37.9 us -> 18.8 us
  other arithmetic: 23.4 us -> 6.9 us
  local copies, waits for them, and re-layouts: 38.3 us -> 22.3 us
  between operations: 13.8 us -> 0.47 us
  loops' own time: 10.5 us -> 0 us
  starting transfers between devices: 17.4 us -> 23.3 us
    all_to_all x1, blocking collectives: 232 us -> 89.4 us  [on_device(): lax.all_to_all(outgoing, ('sp', 'tp'), split_axis=0, concat_axis=0, tiled...]
    pallas_call x0 -> x3, Pallas kernels: none -> 82.5 us  [the longest x1 53.4 us: gather(): pl.pallas_call(gather_kernel, out_shape=(jax.ShapeDtypeStruct((4, 4, 4, 2...]
    all_gather x1 -> x0, waiting for transfers between devices: 68.5 us -> none  [sent_together_2(): out = lax.all_gather(both, axis, axis=dim, tiled=True)]
    dot_general x6 -> x2, matrix products: 20.5 us -> 1.46 us  [the longest x1 0.73 us: on_device(): lax.dot_general(attn_large, weight_large, (((0,), (0,)), ((), ())), prefe...]
    ppermute x0 -> x7, starting transfers between devices: none -> 17.7 us  [the longest x3 12.4 us: on_device(): far_s, far_l, far_ml = [lax.ppermute(a, 'sp', to_late) for a in far]]
    all_to_all x1 -> x0, waiting for transfers between devices: 12.8 us -> none  [sent_to_all(): lax.all_to_all(jnp.broadcast_to(array[None], (devices, *array.shape)), ax...]
    all_to_all x1 -> x0, starting transfers between devices: 12 us -> none  [sent_to_all(): lax.all_to_all(jnp.broadcast_to(array[None], (devices, *array.shape)), ax...]
    split x2 -> x0, local copies, waits for them, and re-layouts: 10.7 us -> none  [sent_together_2(): jnp.split(out, [sum(widths[:k]) for k in range(1, len(widths))], axis=along)]
  transfers between devices with their start and end apart: 3 -> 8, of which waited for: 3 -> 2; matrix products, arithmetic and copies ran while one was open for 2% -> 2% of each run, Pallas kernels for 0% -> 20%
where the time goes in v1:
time: 290 us; the launch traced here: 289 us
  blocking collectives  94.6 us (33%)
  Pallas kernels  82.5 us (28%)
  waiting for transfers between devices  39.9 us (14%)
  starting transfers between devices  23.3 us (8%)
  local copies, waits for them, and re-layouts  22.3 us (8%)
  matrix products  18.8 us (6%)
  other arithmetic  6.9 us (2%)
    all_to_all x1, blocking collectives, on_device(): lax.all_to_all(outgoing, ('sp', 'tp'), split_axis=0, concat_axis=0, tiled...  89.4 us
    pallas_call x1, Pallas kernels, gather(): pl.pallas_call(gather_kernel, out_shape=(jax.ShapeDtypeStruct((4, 4, 4, 2...  53.4 us
    all_to_all x1, waiting for transfers between devices, on_device(): lax.all_to_all(expert_out.reshape(received.shape), ('sp', 'tp'), split_ax...  30.2 us
    pallas_call x2, Pallas kernels, attention(): pl.pallas_call(functools.partial(attention_kernel, diagonal=diagonal), ou...  29.2 us
    ppermute x3, starting transfers between devices, on_device(): far_s, far_l, far_ml = [lax.ppermute(a, 'sp', to_late) for a in far]  12.4 us
    dot_general x1, matrix products, on_device(): jnp.dot(hidden, w_down[0], preferred_element_type=jnp.float32)  9.92 us
    ppermute x3, waiting for transfers between devices, on_device(): far_s, far_l, far_ml = [lax.ppermute(a, 'sp', to_late) for a in far]  9.7 us
    unnamed x31, local copies, waits for them, and re-layouts  7.79 us
  transfers between devices with their start and end apart: 8, of which 2 were waited for; matrix products, arithmetic and copies ran while one was open for 2% of the time, Pallas kernels for 20%

profile of v1, /device:TPU:1, one launch (start us, length us, event | category | flops | bytes accessed | tf_op | source)
XLA Modules:
  0.0 288.9 jit_solution(17249913247609071507)
XLA Ops:
  0.0 0.0 copy-start
  0.0 0.7 broadcast_multiply_fusion
  0.7 0.7 pad_maximum_fusion.2
  1.5 1.5 collective-permute-start
  2.9 0.7 pad_maximum_fusion.1.cq_ref
  3.7 1.3 collective-permute-start.3
  4.9 1.0 reshape.136
  6.0 0.2 copy.25
  6.2 1.3 collective-permute-start.2
  7.5 1.1 copy.23
  8.6 1.3 collective-permute-start.1
  10.0 0.0 copy-done.7
  10.0 0.1 copy.28
  10.2 0.2 fusion.30
  10.4 0.1 add_add_fusion
  10.5 0.2 fusion.32
  10.7 0.1 fusion.29
  10.8 0.1 add_add_fusion.2.bounds
  10.9 0.1 add_add_fusion.1.bounds
  11.0 0.0 collective-permute-done
  11.0 53.4 %gather_keys.1 = (bf16[4,4,4,2,128,384]{5,4,3,2,1,0:T(8,128)(2,1)S(1)}, f32[4,4,4,2,24,128]{5,4,3,2,1,0:T(8,128)S(1)}) custom-call(bf16[128,384]{1,0:T(8,128)(2,1)S(1)} %pad_maximum_fusion.kv_ref, f32[24,128]{1,0:T(8,128)S(1)} %maximum_select_fusion.cum_ref), custom_call_target="tpu_custom_call" | custom-call | tf_op jit(solution)/shard_map/gather_keys/pallas_call | solution.py:139
  64.4 4.5 %copy-done.2 = bf16[4,4,4,2,128,384]{5,4,3,2,1,0:T(8,128)(2,1)} copy-done((bf16[4,4,4,2,128,384]{5,4,3,2,1,0:T(8,128)(2,1)}, bf16[4,4,4,2,128,384]{5,4,3,2,1,0:T(8,128)(2,1)S(1)}, u32[]{:S(2)}) %copy-start.2) | copy-done | bytes 12582936
  68.9 0.0 collective-permute-done.3.cq_ref
  68.9 0.0 collective-permute-done.2.ql_ref
  68.9 0.0 collective-permute-done.1.qs_ref
  68.9 23.4 %attention_far.1 = (bf16[512,256]{1,0:T(8,128)(2,1)S(1)}, bf16[512,256]{1,0:T(8,128)(2,1)S(1)}, f32[32,256]{1,0:T(8,128)S(1)}) custom-call(s32[4]{0:T(128)S(1)} %add_add_fusion.2.bounds, bf16[64,2048]{1,0:T(8,128)(2,1)S(1)} %collective-permute-done.1.qs_ref, bf16[128,1024]{1,0:T(8,128)(2,1)S(1)} %collective-permute-done.2.ql_ref, ...), custom_call_target="tpu_custom_call" | custom-call | flops 8000000000 | bytes 12000000 | tf_op jit(solution)/shard_map/attention_far/pallas_call | solution.py:289
  92.3 1.3 collective-permute-start.4
  93.6 0.0 copy-start.4
  93.6 5.8 %attention_own.1 = (f32[512,256]{1,0:T(8,128)S(1)}, f32[512,256]{1,0:T(8,128)S(1)}, f32[32,256]{1,0:T(8,128)S(1)}) custom-call(s32[4]{0:T(128)S(1)} %add_add_fusion.1.bounds, bf16[64,2048]{1,0:T(8,128)(2,1)S(1)} %bitcast.78, bf16[128,1024]{1,0:T(8,128)(2,1)S(1)} %bitcast.76, f32[16,256]{1,0:T(8,128)S(1)} %pad_maximum_fusion.1.cq_ref, ...), custom_call_target="tpu_custom_call" | custom-call | flops 12000000000 | bytes 12000000 | tf_op jit(solution)/shard_map/attention_own/pallas_call | solution.py:289
  99.4 9.8 %collective-permute-start.5 = (bf16[512,256]{1,0:T(8,128)(2,1)S(1)}, bf16[512,256]{1,0:T(8,128)(2,1)S(1)}, u32[]{:S(2)}, u32[]{:S(2)}) collective-permute-start(bf16[512,256]{1,0:T(8,128)(2,1)S(1)} %get-tuple-element.18), channel_id=1, source_target_pairs={{0,126},{2,124},{4,122},{6,120},{8,118},{10,116},{12,114},{14,112}... | collective-permute-start | bytes 786440 | tf_op jit(solution)/shard_map/ppermute | solution.py:384
  109.3 1.3 collective-permute-start.6
  110.6 0.0 collective-permute-done.4
  110.7 9.7 %collective-permute-done.6 = bf16[512,256]{1,0:T(8,128)(2,1)S(1)} collective-permute-done((bf16[512,256]{1,0:T(8,128)(2,1)S(1)}, bf16[512,256]{1,0:T(8,128)(2,1)S(1)}, u32[]{:S(2)}, u32[]{:S(2)}) %collective-permute-start.6) | collective-permute-done | bytes 262176 | tf_op jit(solution)/shard_map/ppermute | solution.py:384
  120.4 0.1 fusion.24
  120.5 0.0 copy-start.5
  120.5 0.7 fusion.10
  121.2 0.0 collective-permute-done.5
  121.2 0.1 fusion.26
  121.3 1.3 copy-done.5
  122.7 0.7 fusion.9
  123.4 5.2 %all_to_all.15 = bf16[2,128,2048]{2,1,0:T(8,128)(2,1)S(1)} all-to-all(bf16[2,128,2048]{2,1,0:T(8,128)(2,1)S(1)} %bitcast.83), channel_id=1, replica_groups=mesh['sp'=64,'tp'=2] {'tp'}, dimensions={0} | all-to-all | bytes 2097152 | tf_op jit(solution)/shard_map/all_to_all | solution.py:328
  128.6 0.2 convert_reduce_fusion
  128.8 0.0 copy-start.10
  128.8 0.2 multiply_reduce_fusion.1
  129.0 0.7 copy-done.6
  129.6 0.0 copy-done.9
  129.7 0.4 fusion.15
  130.0 0.0 copy-done.10
  130.0 0.8 convolution_convert_fusion
  130.8 2.2 reshape.144
  133.1 89.4 %all_to_all.16 = bf16[128,4,2048]{2,1,0:T(4,128)(2,1)S(1)} all-to-all(bf16[128,4,2048]{2,1,0:T(4,128)(2,1)} %reshape.144), channel_id=1, replica_groups=mesh['sp'=64,'tp'=2] {'sp','tp'}, dimensions={0} | all-to-all | bytes 4194304 | tf_op jit(solution)/shard_map/all_to_all | solution.py:418
  222.4 2.0 reshape.145
  224.5 6.6 %fusion.4 = f32[512,1024]{1,0:T(8,128)} fusion(bf16[512,2048]{1,0:T(8,128)(2,1)} %reshape.145, bf16[1,2048,1024]{2,1,0:T(8,128)(2,1)} %param.29), kind=kOutput, calls=%fused_computation.5 | convolution fusion | flops 2147483648 | bytes 8388608 | tf_op jit(solution)/shard_map/dot_general | solution.py:421
  231.1 9.9 %fusion.6 = bf16[512,2048]{1,0:T(8,128)(2,1)} fusion(bf16[1,1024,2048]{2,1,0:T(8,128)(2,1)} %param.31, f32[512,1024]{1,0:T(8,128)} %fusion.4, bf16[512,2048]{1,0:T(8,128)(2,1)S(1)} %copy-done.3, bf16[1,2048,1024]{2,1,0:T(8,128)(2,1)} %param.30), kind=kOutput, calls=%fused_computation.7 | convolution fusion | flops 4299161600 | bytes 14680064 | tf_op jit(solution)/shard_map/dot_general | solution.py:424
  241.0 4.1 %reshape.146 = bf16[128,4,2048]{2,1,0:T(4,128)(2,1)} reshape(bf16[512,2048]{1,0:T(8,128)(2,1)} %fusion.6) | data formatting | bytes 4194304 | tf_op jit(solution)/shard_map/reshape | solution.py:426
  245.1 5.6 %all-to-all-start.2 = ((bf16[128,4,2048]{2,1,0:T(4,128)(2,1)}), bf16[128,4,2048]{2,1,0:T(4,128)(2,1)}, u32[]{:S(2)}, u32[]{:S(2)}) async-start(bf16[128,4,2048]{2,1,0:T(4,128)(2,1)} %reshape.146), calls=%async_computation.2 | async-start | bytes 4194304 | tf_op jit(solution)/shard_map/all_to_all | solution.py:425
  250.8 30.2 %all-to-all-done.2 = bf16[128,4,2048]{2,1,0:T(4,128)(2,1)} async-done(((bf16[128,4,2048]{2,1,0:T(4,128)(2,1)}), bf16[128,4,2048]{2,1,0:T(4,128)(2,1)}, u32[]{:S(2)}, u32[]{:S(2)}) %all-to-all-start.2) | async-done | bytes 2097184 | tf_op jit(solution)/shard_map/all_to_all | solution.py:425
  281.0 2.5 reshape.147
  283.5 2.3 gather_fusion
  285.9 1.5 convert_element_type.71
  287.3 0.0 copy-start.1
  287.3 0.3 multiply_reduce_fusion
  287.7 1.2 fusion.18
  288.9 0.0 copy-done.1
  (41 shorter events, 0.3 us)
Async XLA Ops:
  0.0 10.0 %copy-start = (bf16[256,256]{1,0:T(8,128)(2,1)S(1)}, bf16[256,256]{1,0:T(8,128)(2,1)}, u32[]{:S(2)}) copy-start(bf16[256,256]{1,0:T(8,128)(2,1)} %param.20) | copy-start | bytes 393220
  0.0 10.0 %copy-start.8 = (bf16[256,128]{1,0:T(8,128)(2,1)S(1)}, bf16[256,128]{1,0:T(8,128)(2,1)}, u32[]{:S(2)}) copy-start(bf16[256,128]{1,0:T(8,128)(2,1)} %param.19) | copy-start | bytes 196612
  0.0 10.0 %copy-start.7 = (s32[2,128]{1,0:T(2,128)S(1)}, s32[2,128]{1,0:T(2,128)}, u32[]{:S(2)}) copy-start(s32[2,128]{1,0:T(2,128)} %param.32) | copy-start | bytes 3076
  1.5 9.5 %collective-permute-start = (f32[12,128]{1,0:T(8,128)S(1)}, f32[12,128]{1,0:T(8,128)S(1)}, u32[]{:S(2)}, u32[]{:S(2)}) collective-permute-start(f32[12,128]{1,0:T(8,128)S(1)} %bitcast.89), channel_id=1, source_target_pairs={{0,1},{1,0},{2,3},{3,2},{4,5},{5,4},{6,7},{7,6},{8,9},{9,8},{10,11... | collective-permute-start | bytes 18440 | tf_op jit(solution)/shard_map/ppermute | solution.py:363
  3.7 65.3 %collective-permute-start.3 = (f32[16,256]{1,0:T(8,128)S(1)}, f32[16,256]{1,0:T(8,128)S(1)}, u32[]{:S(2)}, u32[]{:S(2)}) collective-permute-start(f32[16,256]{1,0:T(8,128)S(1)} %pad_maximum_fusion.1.cq_ref), channel_id=1, source_target_pairs={{126,0},{124,2},{122,4},{120,6},{118,8},{116,10},{114,12},{112,14}... | collective-permute-start | bytes 49160 | tf_op jit(solution)/shard_map/ppermute | solution.py:373
  6.2 62.7 %collective-permute-start.2 = (bf16[128,1024]{1,0:T(8,128)(2,1)S(1)}, bf16[128,1024]{1,0:T(8,128)(2,1)S(1)}, u32[]{:S(2)}, u32[]{:S(2)}) collective-permute-start(bf16[128,1024]{1,0:T(8,128)(2,1)S(1)} %bitcast.75), channel_id=1, source_target_pairs={{126,0},{124,2},{122,4},{120,6},{118,8},{116,10},{114,12},{112,14}... | collective-permute-start | bytes 786440 | tf_op jit(solution)/shard_map/ppermute | solution.py:373
  8.6 60.3 %collective-permute-start.1 = (bf16[64,2048]{1,0:T(8,128)(2,1)S(1)}, bf16[64,2048]{1,0:T(8,128)(2,1)S(1)}, u32[]{:S(2)}, u32[]{:S(2)}) collective-permute-start(bf16[64,2048]{1,0:T(8,128)(2,1)S(1)} %bitcast.77), channel_id=1, source_target_pairs={{126,0},{124,2},{122,4},{120,6},{118,8},{116,10},{114,12},{112,14}... | collective-permute-start | bytes 786440 | tf_op jit(solution)/shard_map/ppermute | solution.py:373
  64.4 4.5 %copy-start.2 = (bf16[4,4,4,2,128,384]{5,4,3,2,1,0:T(8,128)(2,1)}, bf16[4,4,4,2,128,384]{5,4,3,2,1,0:T(8,128)(2,1)S(1)}, u32[]{:S(2)}) copy-start(bf16[4,4,4,2,128,384]{5,4,3,2,1,0:T(8,128)(2,1)S(1)} %get-tuple-element.13) | copy-start | bytes 37748740
  92.3 18.3 %collective-permute-start.4 = (f32[32,256]{1,0:T(8,128)S(1)}, f32[32,256]{1,0:T(8,128)S(1)}, u32[]{:S(2)}, u32[]{:S(2)}) collective-permute-start(f32[32,256]{1,0:T(8,128)S(1)} %get-tuple-element.17), channel_id=1, source_target_pairs={{0,126},{2,124},{4,122},{6,120},{8,118},{10,116},{12,114},{14,112}... | collective-permute-start | bytes 98312 | tf_op jit(solution)/shard_map/ppermute | solution.py:384
  93.6 26.8 %copy-start.4 = (bf16[1024,2048]{1,0:T(8,128)(2,1)S(1)}, bf16[1024,2048]{1,0:T(8,128)(2,1)}, u32[]{:S(2)}) copy-start(bf16[1024,2048]{1,0:T(8,128)(2,1)} %param.25) | copy-start | bytes 12582916
  99.4 21.8 %collective-permute-start.5 = (bf16[512,256]{1,0:T(8,128)(2,1)S(1)}, bf16[512,256]{1,0:T(8,128)(2,1)S(1)}, u32[]{:S(2)}, u32[]{:S(2)}) collective-permute-start(bf16[512,256]{1,0:T(8,128)(2,1)S(1)} %get-tuple-element.18), channel_id=1, source_target_pairs={{0,126},{2,124},{4,122},{6,120},{8,118},{10,116},{12,114},{14,112}... | collective-permute-start | bytes 786440 | tf_op jit(solution)/shard_map/ppermute | solution.py:384
  109.3 11.1 %collective-permute-start.6 = (bf16[512,256]{1,0:T(8,128)(2,1)S(1)}, bf16[512,256]{1,0:T(8,128)(2,1)S(1)}, u32[]{:S(2)}, u32[]{:S(2)}) collective-permute-start(bf16[512,256]{1,0:T(8,128)(2,1)S(1)} %get-tuple-element.20), channel_id=1, source_target_pairs={{0,126},{2,124},{4,122},{6,120},{8,118},{10,116},{12,114},{14,112}... | collective-permute-start | bytes 786440 | tf_op jit(solution)/shard_map/ppermute | solution.py:384
  120.5 2.2 copy-start.5
  128.6 1.0 copy-start.6
  128.6 1.0 copy-start.9
  128.8 1.2 copy-start.10
  224.5 6.6 %copy-start.3 = (bf16[512,2048]{1,0:T(8,128)(2,1)S(1)}, bf16[512,2048]{1,0:T(8,128)(2,1)}, u32[]{:S(2)}) copy-start(bf16[512,2048]{1,0:T(8,128)(2,1)} %reshape.145) | copy-start | bytes 6291460
  245.1 5.6 %copy-start.12 = (f32[128]{0:T(128)S(1)}, f32[128]{0:T(128)}, u32[]{:S(2)}) copy-start(f32[128]{0:T(128)} %param.33) | copy-start | bytes 1540
  245.1 35.9 %all-to-all-start.2 = ((bf16[128,4,2048]{2,1,0:T(4,128)(2,1)}), bf16[128,4,2048]{2,1,0:T(4,128)(2,1)}, u32[]{:S(2)}, u32[]{:S(2)}) async-start(bf16[128,4,2048]{2,1,0:T(4,128)(2,1)} %reshape.146), calls=%async_computation.2 | async-start | bytes 4194304 | tf_op jit(solution)/shard_map/all_to_all | solution.py:425
  285.9 1.8 copy-start.11
  287.3 1.5 copy-start.1

commit v2 on v1

v2 whole, which is shorter than its diff:
```python
import functools
import math

import jax
import jax.numpy as jnp
from jax import lax
from jax.experimental import pallas as pl
from jax.experimental.pallas import tpu as pltpu
from jax.sharding import PartitionSpec as P


MESH = pl.DeviceIdType.MESH
norm_eps = 1e-06
far_score = -1e30
log2e = 1.4426950408889634
f32, bf16 = jnp.float32, jnp.bfloat16
unit = 1024
own_units = 9

orders = (("x", "y", "z"), ("y", "z", "x"), ("z", "x", "y"))
pieces = (
    (0, 0, 0, 32, 16),
    (1, 0, 48, 32, 16),
    (2, 0, 96, 32, 16),
    (0, 0, 32, 16, 8),
    (1, 0, 80, 16, 8),
    (2, 1, 0, 32, 16),
)
shift = (3, 1, 2, 2)


def gather_kernel(small_ref, large_ref, gates_ref, qs_ref, ql_ref, g_ref, c_ref, far_qs, far_ql, far_gates,
                  send, recv, dsend, drecv, far_send, far_recv):
    sp, tp = lax.axis_index("sp"), lax.axis_index("tp")
    at = {"z": sp // 16, "y": (sp // 4) % 4, "x": sp % 4}
    partner = (sp, 1 - tp)
    mirror = (63 - sp, tp)
    far_qs[...] = jnp.zeros(far_qs.shape, bf16)
    far_ql[...] = jnp.zeros(far_ql.shape, bf16)
    far_gates[...] = jnp.zeros(far_gates.shape, f32)

    def moved(dim, by):
        here = dict(at)
        here[dim] = (at[dim] + by) % 4
        return (here["z"] * 16 + here["y"] * 4 + here["x"], tp)

    barrier = pltpu.get_barrier_semaphore()
    for dim in ("x", "y", "z"):
        for by in (1, 3):
            pl.semaphore_signal(barrier, inc=1, device_id=moved(dim, by), device_id_type=MESH)
    pl.semaphore_signal(barrier, inc=1, device_id=partner, device_id_type=MESH)
    pl.semaphore_signal(barrier, inc=1, device_id=mirror, device_id_type=MESH)

    for half in (0, 1):
        rows = slice(half * 128, half * 128 + 128)
        g_ref[at["z"], at["y"], at["x"], half, :, 0:128] = small_ref[rows, :]
        g_ref[at["z"], at["y"], at["x"], half, :, 128:384] = large_ref[rows, :]
        c_ref[at["z"], at["y"], at["x"], half * 16 : half * 16 + 16, :] = gates_ref[:, rows]

    def rows_of(piece, kind):
        _, _, first, count, half = pieces[piece]
        if kind == 2:
            return (first, half)
        if kind == 3:
            return (first + half, count - half)
        return (first, count)

    def view(piece, phase, offset, kind, side):
        order = orders[pieces[piece][0]]
        index = []
        for dim in ("z", "y", "x"):
            where = order.index(dim)
            if where < phase:
                index.append(slice(None))
            else:
                index.append((at[dim] + offset) % 4 if where == phase else at[dim])
        rows = pl.ds(*rows_of(piece, kind))
        if pieces[piece][1]:
            return c_ref.at[(*index, rows, slice(None))]
        return g_ref.at[(*index, side, rows, slice(None))]

    def sent(piece, phase, kind):
        target = view(piece, phase, (0, 0, 3, 1)[kind], kind, tp)
        return pltpu.make_async_remote_copy(
            src_ref=target, dst_ref=target, send_sem=send.at[piece, phase, kind], recv_sem=recv.at[piece, phase, kind],
            device_id=moved(orders[pieces[piece][0]][phase], 1 if kind in (0, 2) else 3), device_id_type=MESH)

    def arrived(piece, phase, kind):
        ref = view(piece, phase, shift[kind], kind, tp)
        return pltpu.make_async_remote_copy(
            src_ref=ref, dst_ref=ref, send_sem=send.at[piece, phase, kind], recv_sem=recv.at[piece, phase, kind],
            device_id=partner, device_id_type=MESH)

    def shared(piece, phase, kind, side):
        ref = view(piece, phase, shift[kind], kind, side)
        return pltpu.make_async_remote_copy(
            src_ref=ref, dst_ref=ref, send_sem=dsend.at[piece, phase, kind], recv_sem=drecv.at[piece, phase, kind],
            device_id=partner, device_id_type=MESH)

    far = [
        pltpu.make_async_remote_copy(
            src_ref=source, dst_ref=target, send_sem=far_send.at[k], recv_sem=far_recv.at[k],
            device_id=mirror, device_id_type=MESH)
        for k, (source, target) in enumerate(((gates_ref, far_gates), (qs_ref, far_qs), (ql_ref, far_ql)))
    ]
    count = range(len(pieces))
    pl.semaphore_wait(barrier, 8)
    for piece in count:
        for kind in (0, 1):
            sent(piece, 0, kind).start()

    @pl.when(sp >= 32)
    def _():
        for copy in far:
            copy.start()

    for phase in range(3):
        for piece in count:
            for kind in (0, 1):
                arrived(piece, phase, kind).wait_recv()
                sent(piece, phase, 2 + kind).start()
                if pieces[piece][1] == 0:
                    shared(piece, phase, kind, tp).start()
        for piece in count:
            for kind in (2, 3):
                arrived(piece, phase, kind).wait_recv()
            if phase < 2:
                for kind in (0, 1):
                    sent(piece, phase + 1, kind).start()
            if pieces[piece][1] == 0:
                for kind in (2, 3):
                    shared(piece, phase, kind, tp).start()

    @pl.when(sp >= 32)
    def _():
        for copy in far:
            copy.wait_send()

    @pl.when(sp < 32)
    def _():
        for copy in far:
            copy.wait_recv()

    for phase in range(3):
        for piece in count:
            for kind in range(4):
                sent(piece, phase, kind).wait_send()
                if pieces[piece][1] == 0:
                    shared(piece, phase, kind, tp).wait_send()
                    shared(piece, phase, kind, 1 - tp).wait_recv()


def gather(small, large, gates, qs, ql):
    DMA = pltpu.SemaphoreType.DMA
    shape = (len(pieces), 3, 4)
    V = pl.BlockSpec(memory_space=pltpu.VMEM)
    return pl.pallas_call(
        gather_kernel,
        out_shape=(
            jax.ShapeDtypeStruct((4, 4, 4, 2, 128, 384), bf16),
            jax.ShapeDtypeStruct((4, 4, 4, 32, 128), f32),
            jax.ShapeDtypeStruct((256, 512), bf16),
            jax.ShapeDtypeStruct((256, 512), bf16),
            jax.ShapeDtypeStruct((16, 256), f32),
        ),
        in_specs=[V] * 5,
        out_specs=(V,) * 5,
        scratch_shapes=[DMA(shape), DMA(shape), DMA(shape), DMA(shape), DMA((3,)), DMA((3,))],
        compiler_params=pltpu.CompilerParams(collective_id=0, has_side_effects=True, vmem_limit_bytes=24 * 1024 * 1024),
        name="gather_keys",
    )(small, large, gates, qs, ql)


def attention_kernel(qs_ref, ql_ref, cq_ref, whole_ref, c_ref, o_ref, ml_ref,
                     near, near_sems, tile, vts, vtl, qs, ql, acc_s, acc_l, top, *, diagonal):
    sp = lax.axis_index("sp")
    if diagonal:
        hi, q0 = sp // 4 + 1, sp * 256
        lo = jnp.maximum(hi - own_units, 0)
    else:
        lo, q0 = 0, (63 - sp) * 256
        hi = jnp.where(sp < 32, jnp.maximum((63 - sp) // 4 + 1 - own_units, 0), 0)

    def fetch(i):
        return pltpu.make_async_copy(
            whole_ref.at[pl.ds(pl.multiple_of((hi - 1 - i) * unit, unit), unit), :], near.at[i], near_sems.at[i])

    if diagonal:
        lax.fori_loop(0, hi - lo, lambda i, _: (fetch(i).start(), 0)[1], 0)
    nq = 256
    cs, cl = log2e / 8.0, log2e / math.sqrt(128.0)
    n = hi - lo

    acc_s[...] = jnp.zeros(acc_s.shape, f32)
    acc_l[...] = jnp.zeros(acc_l.shape, f32)
    top[...] = jnp.zeros(top.shape, f32)
    vts[64:80, :] = jnp.ones((16, unit), bf16)
    vtl[128:144, :] = jnp.ones((16, unit), bf16)
    for k in range(4):
        w = slice(k * nq, (k + 1) * nq)
        two = qs_ref[:, k * 128 : (k + 1) * 128].T
        qs[128:192, 2 * k * nq : (2 * k + 1) * nq] = two[0:64, :]
        qs[128:192, (2 * k + 1) * nq : (2 * k + 2) * nq] = two[64:128, :]
        ql[0:128, w] = ql_ref[:, k * 128 : (k + 1) * 128].T
    qs[192:256, :] = jnp.zeros((64, 2048), bf16)
    row = lax.broadcasted_iota(jnp.int32, (128, nq), 0)
    for h in range(12):
        here = cq_ref[h : h + 1, :]
        high = here.astype(bf16).astype(f32)
        rest = here - high
        middle = rest.astype(bf16).astype(f32)
        low = rest - middle
        chosen = jnp.where((row == h) | (row == 16 + h) | (row == 32 + h), -8.0, 0.0)
        chosen = jnp.where(row == 48, 8.0 * high, chosen)
        chosen = jnp.where(row == 49, 8.0 * middle, chosen)
        chosen = jnp.where(row == 50, 8.0 * low, chosen).astype(bf16)
        if h < 8:
            qs[0:128, h * nq : (h + 1) * nq] = chosen
        else:
            ql[128:256, (h - 8) * nq : (h - 7) * nq] = chosen
    size_s = jnp.max(jnp.sum(jnp.abs(qs[128:192, :].astype(f32)), axis=0, keepdims=True))
    size_l = jnp.max(jnp.sum(jnp.abs(ql[0:128, :].astype(f32)), axis=0, keepdims=True))
    bounded = (size_s <= 150.0) & (size_l <= 210.0)

    def ready(i):
        u = hi - 1 - i
        if diagonal:
            fetch(i).wait()
            here = near.at[i]
        else:
            here = whole_ref.at[pl.ds(pl.multiple_of(u * unit, unit), unit), :]
        for j in range(8):
            gate = c_ref[u * 4 + j // 2, (j % 2) * 16 : (j % 2) * 16 + 16, :]
            high = gate.astype(bf16).astype(f32)
            rest = gate - high
            middle = rest.astype(bf16).astype(f32)
            wide = jnp.concatenate([high, middle, rest - middle, jnp.ones((8, 128), f32), jnp.zeros((72, 128), f32)], axis=0)
            tile[j * 128 : (j + 1) * 128, :] = wide.T.astype(bf16)
        vts[0:64, :] = here[:, 0:128].T[64:128, :]
        vtl[0:128, :] = here[:, 256:384].T
        return u, here

    def keys_small(here):
        return jnp.concatenate([tile[...], here[:, 0:128]], axis=1)

    def keys_large(here):
        return jnp.concatenate([here[:, 128:256], tile[...]], axis=1)

    def allowed(u, width):
        key = u * unit + lax.broadcasted_iota(jnp.int32, (unit, width), 0)
        query = q0 + (lax.broadcasted_iota(jnp.int32, (unit, width), 1) & (nq - 1))
        return key <= query

    def quick(i, masked):
        u, here = ready(i)
        for keys, q, w, vt, acc, scale in (
            (keys_small, qs, 0, vts, acc_s, cs),
            (keys_small, qs, 1024, vts, acc_s, cs),
            (keys_large, ql, 0, vtl, acc_l, cl),
        ):
            s = jnp.dot(keys(here), q[:, w : w + 1024], preferred_element_type=f32) * scale
            if masked:
                s = jnp.where(allowed(u, 1024), s, far_score)
            p = jnp.exp2(s).astype(bf16)
            acc[:, w : w + 1024] += jnp.dot(vt[...], p, preferred_element_type=f32)

    def careful(i, _):
        u, here = ready(i)

        def group(keys, q, vt, acc, scale, count, base):
            def head(h, _):
                w = pl.ds(pl.multiple_of(h * nq, nq), nq)
                s = jnp.dot(keys(here), q[:, w], preferred_element_type=f32) * scale
                s = jnp.where(allowed(u, nq), s, far_score)
                before = top[base + h]
                after = jnp.maximum(before, jnp.max(s, axis=0, keepdims=True))
                top[base + h] = after
                p = jnp.exp2(s - after).astype(bf16)
                acc[:, w] = acc[:, w] * jnp.exp2(before - after) + jnp.dot(vt[...], p, preferred_element_type=f32)
                return 0

            lax.fori_loop(0, count, head, 0)

        group(keys_small, qs, vts, acc_s, cs, 8, 0)
        group(keys_large, ql, vtl, acc_l, cl, 4, 8)
        return 0

    @pl.when(bounded)
    def _():
        if diagonal:
            quick(0, True)
        lax.fori_loop(1 if diagonal else 0, n, lambda i, _: (quick(i, False), 0)[1], 0)

    @pl.when(jnp.logical_not(bounded))
    def _():
        top[...] = jnp.full(top.shape, far_score, f32)
        lax.fori_loop(0, n, careful, 0)

    ml_ref[...] = jnp.zeros(ml_ref.shape, f32)
    for h in range(12):
        size, acc, base, k = (64, acc_s, 0, h) if h < 8 else (128, acc_l, 512, h - 8)
        w = slice(k * nq, (k + 1) * nq)
        total = acc[size : size + 1, w]
        scale = jnp.where(total > 0, 1.0 / jnp.where(total > 0, total, 1.0), 0.0)
        o_ref[base + k * size : base + (k + 1) * size, :] = (acc[0:size, w] * scale).astype(o_ref.dtype)
        ml_ref[h : h + 1, :] = top[h]
        ml_ref[16 + h : 17 + h, :] = total


def attention(qs, ql, cq, g, c, diagonal):
    V = pl.BlockSpec(memory_space=pltpu.VMEM)
    kind = f32 if diagonal else bf16
    VM = pltpu.VMEM
    return pl.pallas_call(
        functools.partial(attention_kernel, diagonal=diagonal),
        out_shape=(
            jax.ShapeDtypeStruct((1024, 256), kind),
            jax.ShapeDtypeStruct((32, 256), f32),
        ),
        in_specs=[V] * 3 + [pl.BlockSpec(memory_space=pltpu.HBM) if diagonal else V, V],
        out_specs=(V, V),
        scratch_shapes=[
            VM((own_units if diagonal else 1, unit, 384), bf16), pltpu.SemaphoreType.DMA((own_units,)), VM((unit, 128), bf16),
            VM((80, unit), bf16), VM((144, unit), bf16), VM((256, 2048), bf16), VM((256, 1024), bf16),
            VM((80, 2048), f32), VM((144, 1024), f32), VM((12, 1, 256), f32),
        ],
        compiler_params=pltpu.CompilerParams(vmem_limit_bytes=36 * 1024 * 1024),
        cost_estimate=pl.CostEstimate(flops=12_000_000_000 if diagonal else 8_000_000_000, bytes_accessed=12_000_000, transcendentals=26_000_000),
        name="attention_own" if diagonal else "attention_far",
    )(qs, ql, cq, g, c)


def merged(own, far, m_own, m_far, l_own, l_far, heads):
    m_far = jnp.where(l_far > 0, m_far, far_score)
    most = jnp.maximum(m_own, m_far)
    a, b = l_own * jnp.exp2(m_own - most), l_far * jnp.exp2(m_far - most)
    whole = a + b
    size = own.shape[0] // heads
    own = own.reshape(heads, size, 256) * (a / whole)[:, None, :]
    far = far.astype(f32).reshape(heads, size, 256) * (b / whole)[:, None, :]
    return (own + far).astype(bf16).reshape(heads * size, 256)


def reach(offset):
    return sum((0, 1, 2, 1)[(offset // step) % 4] for step in (1, 4, 16))


offsets = tuple(sorted(range(1, 64), key=lambda offset: -reach(offset)))


def expert_kernel(part_ref, residual_ref, mix_ref, route_ref, blend_ref, table_ref, weight_ref, gate_hbm, up_hbm, down_hbm, out_ref,
                  gate_w, up_w, down_w, other, rows, leaving, taken, hidden, made, back, kept, given, swapped,
                  load, pair_send, pair_recv, go_send, go_recv, back_send, back_recv):
    sp, tp = lax.axis_index("sp"), lax.axis_index("tp")
    z, y, x = sp // 16, (sp // 4) % 4, sp % 4

    def chip(offset, sign):
        oz, oy, ox = offset // 16, (offset // 4) % 4, offset % 4
        return ((z + sign * oz + 4) % 4) * 16 + ((y + sign * oy + 4) % 4) * 4 + (x + sign * ox + 4) % 4

    partner = (sp, 1 - tp)
    loads = [
        pltpu.make_async_copy(source.at[0], target, load.at[k])
        for k, (source, target) in enumerate(((gate_hbm, gate_w), (up_hbm, up_w), (down_hbm, down_w)))
    ]
    barrier = pltpu.get_barrier_semaphore()
    for offset in offsets:
        pl.semaphore_signal(barrier, inc=1, device_id=(chip(offset, 1), tp), device_id_type=MESH)
    pl.semaphore_signal(barrier, inc=1, device_id=partner, device_id_type=MESH)
    for copy in loads:
        copy.start()
    pl.semaphore_wait(barrier, 64)

    def across(source, target, k):
        return pltpu.make_async_remote_copy(
            src_ref=source, dst_ref=target, send_sem=pair_send.at[k], recv_sem=pair_recv.at[k],
            device_id=partner, device_id_type=MESH)

    first = across(part_ref.at[pl.ds((1 - tp) * 128, 128), :], other, 0)
    first.start()
    first.wait()

    def scaled(values, gain):
        return values * lax.rsqrt(jnp.mean(values * values, axis=-1, keepdims=True) + norm_eps) * gain

    mixer = part_ref[pl.ds(pl.multiple_of(tp * 128, 128), 128), :].astype(f32) + other[...].astype(f32)
    mixed = (residual_ref[...].astype(f32) + scaled(mixer, mix_ref[...])).astype(bf16)
    kept[...] = mixed
    given[...] = scaled(mixed.astype(f32), route_ref[...]).astype(bf16)
    mine = pl.ds(pl.multiple_of(tp * 128, 128), 128)
    rows[mine, :] = given[...]
    second = across(given, rows.at[mine, :], 1)
    second.start()
    second.wait_send()
    theirs = rows.at[pl.ds(pl.multiple_of((1 - tp) * 128, 128), 128), :]
    across(theirs, theirs, 1).wait_recv()
    for w in range(0, 2048, 512):
        leaving[:, :, w : w + 512] = jnp.dot(table_ref[...], rows[:, w : w + 512], preferred_element_type=f32).astype(bf16).reshape(64, 8, 512)

    def go(n):
        return pltpu.make_async_remote_copy(
            src_ref=leaving.at[chip(offsets[n], 1)], dst_ref=taken.at[n], send_sem=go_send.at[n], recv_sem=go_recv.at[n],
            device_id=(chip(offsets[n], 1), tp), device_id_type=MESH)

    def come(n):
        return pltpu.make_async_remote_copy(
            src_ref=made.at[n], dst_ref=back.at[sp], send_sem=back_send.at[n], recv_sem=back_recv.at[n],
            device_id=(chip(offsets[n], -1), tp), device_id_type=MESH)

    def came(n):
        ref = back.at[chip(offsets[n], 1)]
        return pltpu.make_async_remote_copy(
            src_ref=ref, dst_ref=ref, send_sem=back_send.at[n], recv_sem=back_recv.at[n], device_id=partner, device_id_type=MESH)

    for n in range(63):
        go(n).start()
    taken[63] = leaving[sp]
    for copy in loads:
        copy.wait()
    for group in (0, 1):
        members = range(32 * group, min(32 * group + 32, 63))
        for n in members:
            go(n).wait_recv()
        arrivals = taken[32 * group : 32 * group + 32].reshape(256, 2048)

        def widen(k, _):
            w = pl.ds(pl.multiple_of(k * 256, 256), 256)
            gated = jnp.dot(arrivals, gate_w[:, w], preferred_element_type=f32)
            upped = jnp.dot(arrivals, up_w[:, w], preferred_element_type=f32)
            hidden[:, w] = (gated / (1.0 + jnp.exp(-gated)) * upped).astype(bf16)
            return 0

        lax.fori_loop(0, 4, widen, 0)

        def narrow(k, _):
            w = pl.ds(pl.multiple_of(k * 512, 512), 512)
            made[32 * group : 32 * group + 32, :, w] = jnp.dot(hidden[...], down_w[:, w], preferred_element_type=f32).astype(bf16).reshape(32, 8, 512)
            return 0

        lax.fori_loop(0, 4, narrow, 0)
        for n in members:
            come(n).start()
    back[sp] = made[63]
    for n in range(63):
        go(n).wait_send()
    for n in range(63):
        came(n).wait_recv()
    for n in range(63):
        come(n).wait_send()
    ours = pl.ds(pl.multiple_of(tp * 128, 128), 128)
    away = pl.ds(pl.multiple_of((1 - tp) * 128, 128), 128)

    for w in range(0, 2048, 512):
        returned = back[:, :, w : w + 512].reshape(512, 512)
        given[:, w : w + 512] = (
            jnp.dot(weight_ref[away, 0:512], returned, preferred_element_type=f32)
            + jnp.dot(weight_ref[away, 512:1024], returned, preferred_element_type=f32)
        ).astype(bf16)
    third = across(given, swapped, 2)
    third.start()
    parts = []
    for w in range(0, 2048, 512):
        returned = back[:, :, w : w + 512].reshape(512, 512)
        parts.append(
            jnp.dot(weight_ref[ours, 0:512], returned, preferred_element_type=f32)
            + jnp.dot(weight_ref[ours, 512:1024], returned, preferred_element_type=f32)
        )
    third.wait()
    blended = jnp.concatenate(parts, axis=1) + swapped[...].astype(f32)
    out_ref[...] = (kept[...].astype(f32) + scaled(blended, blend_ref[...])).astype(bf16)


def experts(part, residual, gain_mix, gain_route, gain_blend, table, weight, w_gate, w_up, w_down):
    V = pl.BlockSpec(memory_space=pltpu.VMEM)
    A = pl.BlockSpec(memory_space=pl.ANY)
    VM, DMA = pltpu.VMEM, pltpu.SemaphoreType.DMA
    return pl.pallas_call(
        expert_kernel,
        out_shape=jax.ShapeDtypeStruct((128, 2048), bf16),
        in_specs=[V] * 7 + [A] * 3,
        out_specs=V,
        scratch_shapes=[
            VM((2048, 1024), bf16), VM((2048, 1024), bf16), VM((1024, 2048), bf16),
            VM((128, 2048), bf16), VM((256, 2048), bf16), VM((64, 8, 2048), bf16), VM((64, 8, 2048), bf16),
            VM((256, 1024), bf16), VM((64, 8, 2048), bf16), VM((64, 8, 2048), bf16),
            VM((128, 2048), bf16), VM((128, 2048), bf16), VM((128, 2048), bf16),
            DMA((3,)), DMA((3,)), DMA((3,)), DMA((64,)), DMA((64,)), DMA((64,)), DMA((64,)),
        ],
        compiler_params=pltpu.CompilerParams(collective_id=1, has_side_effects=True, vmem_limit_bytes=50 * 1024 * 1024),
        name="experts",
    )(part, residual, gain_mix, gain_route, gain_blend, table, weight, w_gate, w_up, w_down)


def routing(route, route_bias, tp):
    def both(a):
        theirs = lax.ppermute(a, "tp", [(0, 1), (1, 0)])
        return jnp.where(tp == 0, jnp.stack([a, theirs]), jnp.stack([theirs, a]))

    ids = both(route).reshape(2, 256)
    bias = both(route_bias)
    marked = (ids[:, :, None] == jnp.arange(128, dtype=jnp.int32)).astype(bf16)
    before = (jnp.arange(256)[:, None] > jnp.arange(256)[None, :]).astype(bf16)
    counts = jnp.einsum("ij,cje->cie", before, marked, preferred_element_type=f32)
    rank = jnp.sum(counts * marked.astype(f32), axis=2).astype(jnp.int32)
    slot = jnp.where(ids % 2 == tp, ids // 2 * 8 + jnp.arange(2, dtype=jnp.int32)[:, None] * 4 + rank, -1).reshape(2, 2, 128)
    places = jnp.arange(512, dtype=jnp.int32)
    to_slot = slot.transpose(1, 0, 2).reshape(2, 256)
    table = ((places[:, None] == to_slot[0][None, :]) | (places[:, None] == to_slot[1][None, :])).astype(bf16)
    share = jnp.stack([jax.nn.sigmoid(bias), jax.nn.sigmoid(-bias)]).reshape(2, 256)
    weight = sum(jnp.where(to_slot[k][:, None] == places[None, :], share[k][:, None], 0.0) for k in range(2))
    high = lax.reduce_precision(weight, 8, 7)
    return table, jnp.concatenate([high, weight - high], axis=1).astype(bf16)


def on_device(
    queries_small,
    queries_large,
    kv_small,
    kv_large,
    cum_small,
    cum_large,
    residual,
    out_small,
    out_large,
    gain_mix,
    gain_route,
    gain_blend,
    w_gate,
    w_up,
    w_down,
    route,
    route_bias,
):
    tp = lax.axis_index("tp")
    chips = lax.axis_size("sp")
    gates = jnp.concatenate([cum_small, cum_large * jnp.float32(math.sqrt(2.0)), jnp.zeros((4, 256), f32)], axis=0)
    to_late = [(i, chips - 1 - i) for i in range(chips // 2)]
    g, c, *far_q = gather(kv_small, kv_large, gates, queries_small, queries_large)
    g, c = g.reshape(chips * 256, 384), c.reshape(chips, 32, 128)
    far_o, far_ml = attention(*far_q, g, c, False)
    far_o = lax.ppermute(far_o, "sp", to_late)
    far_ml = lax.ppermute(far_ml, "sp", to_late)
    own_o, own_ml = attention(queries_small, queries_large, gates, g, c, True)
    attn_small = merged(own_o[0:512], far_o[0:512], own_ml[0:8], far_ml[0:8], own_ml[16:24], far_ml[16:24], 8)
    attn_large = merged(own_o[512:], far_o[512:], own_ml[8:12], far_ml[8:12], own_ml[24:28], far_ml[24:28], 4)
    weight_small = lax.dynamic_slice_in_dim(
        out_small, tp * 512, 512, 0
    )
    weight_large = lax.dynamic_slice_in_dim(
        out_large, tp * 512, 512, 0
    )
    part = (
        lax.dot_general(attn_small, weight_small, (((0,), (0,)), ((), ())), preferred_element_type=f32)
        + lax.dot_general(attn_large, weight_large, (((0,), (0,)), ((), ())), preferred_element_type=f32)
    ).astype(bf16)
    table, weight = routing(route, route_bias, tp)
    return experts(
        part, residual, gain_mix[None], gain_route[None], gain_blend[None], table, weight, w_gate, w_up, w_down
    )


def solution(mesh):
    in_specs = (
        P("sp", "tp"),
        P("sp", "tp"),
        P("sp", None),
        P("sp", None),
        P("tp", "sp"),
        P("tp", "sp"),
        P(("sp", "tp"), None),
        P(),
        P(),
        P(),
        P(),
        P(),
        P(("sp", "tp"), None, None),
        P(("sp", "tp"), None, None),
        P(("sp", "tp"), None, None),
        P(None, ("sp", "tp")),
        P(("sp", "tp")),
    )
    out_specs = P(("sp", "tp"), None)
    return jax.shard_map(
        on_device, mesh=mesh, in_specs=in_specs, out_specs=out_specs, check_vma=False
    )
```

time: 290 us -> 226 us (0.78)
  Pallas kernels: 82.5 us -> 207 us
  blocking collectives: 94.6 us -> 0 us
  waiting for transfers between devices: 39.9 us -> 0.67 us
  starting transfers between devices: 23.3 us -> 3.29 us
  matrix products: 18.8 us -> 3.36 us
  local copies, waits for them, and re-layouts: 22.3 us -> 9.1 us
  other arithmetic: 6.9 us -> 2.13 us
    pallas_call x0 -> x1, Pallas kernels: none -> 125 us  [experts(): pl.pallas_call(expert_kernel, out_shape=jax.ShapeDtypeStruct((128, 2048),...]
    all_to_all x2 -> x0, blocking collectives: 94.6 us -> none  [the longest x1 89.4 us: on_device(): lax.all_to_all(outgoing, ('sp', 'tp'), split_axis=0, concat_axis=0, tiled...]
    all_to_all x1 -> x0, waiting for transfers between devices: 30.2 us -> none  [on_device(): lax.all_to_all(expert_out.reshape(received.shape), ('sp', 'tp'), split_ax...]
    dot_general x3 -> x1, matrix products: 17.3 us -> 0.25 us  [routing(): jnp.einsum('ij,cje->cie', before, marked, preferred_element_type=f32)]
    ppermute x7 -> x4, starting transfers between devices: 17.7 us -> 3.29 us  [the longest x1 1.32 us: on_device(): far_o = lax.ppermute(far_o, 'sp', to_late)]
    reshape x8 -> x0, local copies, waits for them, and re-layouts: 12.2 us -> none  [the longest x1 4.09 us: on_device(): expert_out.reshape(received.shape)]
    ppermute x7 -> x4, waiting for transfers between devices: 9.71 us -> 0.67 us  [the longest x1 0.67 us: on_device(): far_o = lax.ppermute(far_o, 'sp', to_late)]
    all_to_all x1 -> x0, starting transfers between devices: 5.6 us -> none  [on_device(): lax.all_to_all(expert_out.reshape(received.shape), ('sp', 'tp'), split_ax...]
  transfers between devices with their start and end apart: 8 -> 4, of which waited for: 2 -> 1; matrix products, arithmetic and copies ran while one was open for 2% -> 0% of each run, Pallas kernels for 20% -> 2%
where the time goes in v2:
time: 226 us
  Pallas kernels  207 us (92%)
  local copies, waits for them, and re-layouts  9.1 us (4%)
  matrix products  3.36 us (1%)
  starting transfers between devices  3.29 us (1%)
    pallas_call x1, Pallas kernels, experts(): pl.pallas_call(expert_kernel, out_shape=jax.ShapeDtypeStruct((128, 2048),...  125 us
    pallas_call x1, Pallas kernels, gather(): pl.pallas_call(gather_kernel, out_shape=(jax.ShapeDtypeStruct((4, 4, 4, 2...  55.5 us
    pallas_call x2, Pallas kernels, attention(): pl.pallas_call(functools.partial(attention_kernel, diagonal=diagonal), ou...  26.7 us
    unnamed x31, local copies, waits for them, and re-layouts  9.07 us
  transfers between devices with their start and end apart: 4, of which 1 were waited for; matrix products, arithmetic and copies ran while one was open for 0% of the time, Pallas kernels for 2%

profile of v2, /device:TPU:1, one launch (start us, length us, event | category | flops | bytes accessed | tf_op | source)
XLA Modules:
  0.0 226.1 jit_solution(8595885561624464514)
XLA Ops:
  0.0 0.7 broadcast_multiply_fusion
  0.7 0.7 pad_maximum_fusion.1.gates_ref.cq_ref
  1.4 0.0 copy-start.1
  1.4 0.9 copy-done.1
  2.3 0.0 copy-start.3
  2.3 0.9 copy-done.3
  3.3 0.0 copy-start.5
  3.3 0.9 copy-done.5
  4.2 0.0 copy-start.6
  4.2 0.8 copy-done.6
  5.0 55.5 %gather_keys.1 = (bf16[4,4,4,2,128,384]{5,4,3,2,1,0:T(8,128)(2,1)S(1)}, f32[4,4,4,32,128]{4,3,2,1,0:T(8,128)S(1)}, bf16[256,512]{1,0:T(8,128)(2,1)S(1)}, bf16[256,512]{1,0:T(8,128)(2,1)S(1)}, f32[16,256]{1,0:T(8,128)S(1)}) custom-call(bf16[256,128]{1,0:T(8,128)(2,1)S(1)} %copy-done.6, bf16[256,256]{1,0:T(8,128)(2,1)S(1)} %copy-done.5, ...), custom_call_target="tpu_custom_call" | custom-call | tf_op jit(solution)/shard_map/gather_keys/pallas_call | solution.py:157
  60.5 0.0 copy-start.10
  60.6 0.0 copy-start.13
  60.6 0.0 copy-start.14
  60.6 0.0 copy-start.2
  60.6 0.0 copy-start.4
  60.6 22.3 %attention_far.1 = (bf16[1024,256]{1,0:T(8,128)(2,1)}, f32[32,256]{1,0:T(8,128)S(1)}) custom-call(bf16[256,512]{1,0:T(8,128)(2,1)S(1)} %get-tuple-element.18.qs_ref, bf16[256,512]{1,0:T(8,128)(2,1)S(1)} %get-tuple-element.19.ql_ref, f32[16,256]{1,0:T(8,128)S(1)} %get-tuple-element.20.cq_ref, bf16[16384,384]{1,0:T(8,128)(2,1)S(1)} %bitcast.53, ...), custom_call_target="tpu_custom_call" | custom-call | flops 8000000000 | bytes 12000000 | tf_op jit(solution)/shard_map/attention_far/pallas_call | solution.py:314
  82.9 0.0 copy-done.10
  82.9 1.3 collective-permute-start
  84.2 1.3 collective-permute-start.1
  85.5 0.0 copy-done.13
  85.5 0.6 collective-permute-start.2
  86.1 0.0 copy-done.14
  86.1 0.1 collective-permute-start.3
  86.2 0.0 copy-done.2
  86.2 0.0 copy-done.4
  86.2 0.0 copy-start.11
  86.2 4.6 %copy-done.11 = bf16[4,4,4,2,128,384]{5,4,3,2,1,0:T(8,128)(2,1)S(1)} copy-done((bf16[4,4,4,2,128,384]{5,4,3,2,1,0:T(8,128)(2,1)S(1)}, bf16[4,4,4,2,128,384]{5,4,3,2,1,0:T(8,128)(2,1)}, u32[]{:S(2)}) %copy-start.11) | copy-done | bytes 12582936
  90.8 4.4 %attention_own.1 = (f32[1024,256]{1,0:T(8,128)S(1)}, f32[32,256]{1,0:T(8,128)S(1)}) custom-call(bf16[256,512]{1,0:T(8,128)(2,1)S(1)} %copy-done.2, bf16[256,512]{1,0:T(8,128)(2,1)S(1)} %copy-done.4, f32[16,256]{1,0:T(8,128)S(1)} %pad_maximum_fusion.1.gates_ref.cq_ref, bf16[16384,384]{1,0:T(8,128)(2,1)S(1)} %bitcast.54, f32[64,32,128]{2,1,0:T(8,128)S(1)} %bitcast.56), custom_call_target="tpu_custom_call" | custom-call | flops 12000000000 | bytes 12000000 | tf_op jit(solution)/shard_map/attention_own/pallas_call | solution.py:314
  95.2 0.0 collective-permute-done.3
  95.3 0.0 collective-permute-done.2
  95.3 0.2 fusion.5
  95.6 0.1 fusion.29
  95.7 0.1 fusion.12.table_ref
  95.8 0.0 copy-start.12
  95.8 0.2 reduce-precision_convert_fusion
  96.0 0.1 pad_maximum_fusion.weight_ref
  96.1 0.0 collective-permute-done
  96.2 0.7 collective-permute-done.1
  96.9 0.2 fusion.8
  97.0 0.0 copy-start
  97.0 0.0 copy-start.7
  97.0 0.0 copy-start.8
  97.1 0.0 copy-start.9
  97.1 2.4 %fusion.2 = f32[256,2048]{1,0:T(8,128)S(1)} fusion(bf16[512,256]{1,0:T(8,128)(2,1)S(1)} %get-tuple-element.28, bf16[1024,2048]{1,0:T(8,128)(2,1)} %param.24, s32[]{:T(128)S(6)} %select_n.73), kind=kOutput, calls=%fused_computation.3 | convolution fusion | flops 536870912 | bytes 4456452 | tf_op jit(solution)/shard_map/dot_general | solution.py:553
  99.5 0.0 copy-done.12
  99.5 0.7 fusion.part_ref
  100.2 0.0 copy-done
  100.2 0.0 copy-done.7
  100.2 0.0 copy-done.8
  100.2 0.0 copy-done.9
  100.2 125.0 %experts.1 = bf16[128,2048]{1,0:T(8,128)(2,1)S(1)} custom-call(bf16[256,2048]{1,0:T(8,128)(2,1)S(1)} %fusion.part_ref, bf16[128,2048]{1,0:T(8,128)(2,1)S(1)} %copy-done, f32[1,2048]{1,0:T(1,128)S(1)} %bitcast.50, f32[1,2048]{1,0:T(1,128)S(1)} %bitcast.51, f32[1,2048]{1,0:T(1,128)S(1)} %bitcast.52, bf16[512,256]{1,0:T(8,128)(2,1)S(1)} %fusion.12.table_ref, ...), custom_call_target="tpu_custom_call" | custom-call | tf_op jit(solution)/shard_map/experts/pallas_call | solution.py:477
  225.3 0.8 copy.19
  (11 shorter events, 0.1 us)
Async XLA Ops:
  1.4 0.9 copy-start.1
  2.3 0.9 copy-start.3
  3.3 0.9 copy-start.5
  4.2 0.8 copy-start.6
  60.5 22.3 %copy-start.10 = (bf16[4,4,4,2,128,384]{5,4,3,2,1,0:T(8,128)(2,1)}, bf16[4,4,4,2,128,384]{5,4,3,2,1,0:T(8,128)(2,1)S(1)}, u32[]{:S(2)}) copy-start(bf16[4,4,4,2,128,384]{5,4,3,2,1,0:T(8,128)(2,1)S(1)} %get-tuple-element.14) | copy-start | bytes 37748740
  60.6 25.0 %copy-start.13 = (s32[2,128]{1,0:T(2,128)S(1)}, s32[2,128]{1,0:T(2,128)}, u32[]{:S(2)}) copy-start(s32[2,128]{1,0:T(2,128)} %param.32) | copy-start | bytes 3076
  60.6 25.5 %copy-start.14 = (f32[128]{0:T(128)S(1)}, f32[128]{0:T(128)}, u32[]{:S(2)}) copy-start(f32[128]{0:T(128)} %param.33) | copy-start | bytes 1540
  60.6 25.6 %copy-start.2 = (bf16[256,512]{1,0:T(8,128)(2,1)S(1)}, bf16[256,512]{1,0:T(8,128)(2,1)}, u32[]{:S(2)}) copy-start(bf16[256,512]{1,0:T(8,128)(2,1)} %qs_ref.3) | copy-start | bytes 786436
  60.6 25.6 %copy-start.4 = (bf16[256,512]{1,0:T(8,128)(2,1)S(1)}, bf16[256,512]{1,0:T(8,128)(2,1)}, u32[]{:S(2)}) copy-start(bf16[256,512]{1,0:T(8,128)(2,1)} %ql_ref.3) | copy-start | bytes 786436
  82.9 13.2 %collective-permute-start = (f32[32,256]{1,0:T(8,128)S(1)}, f32[32,256]{1,0:T(8,128)S(1)}, u32[]{:S(2)}, u32[]{:S(2)}) collective-permute-start(f32[32,256]{1,0:T(8,128)S(1)} %get-tuple-element.21), channel_id=1, source_target_pairs={{0,126},{2,124},{4,122},{6,120},{8,118},{10,116},{12,114},{14,112}... | collective-permute-start | bytes 98312 | tf_op jit(solution)/shard_map/ppermute | solution.py:542
  84.2 12.7 %collective-permute-start.1 = (bf16[1024,256]{1,0:T(8,128)(2,1)}, bf16[1024,256]{1,0:T(8,128)(2,1)S(1)}, u32[]{:S(2)}, u32[]{:S(2)}) collective-permute-start(bf16[1024,256]{1,0:T(8,128)(2,1)} %get-tuple-element.22), channel_id=1, source_target_pairs={{0,126},{2,124},{4,122},{6,120},{8,118},{10,116},{12,114},{14,112}... | collective-permute-start | bytes 1572872 | tf_op jit(solution)/shard_map/ppermute | solution.py:541
  85.5 9.7 %collective-permute-start.2 = (s32[2,128]{1,0:T(2,128)S(1)}, s32[2,128]{1,0:T(2,128)S(1)}, u32[]{:S(2)}, u32[]{:S(2)}) collective-permute-start(s32[2,128]{1,0:T(2,128)S(1)} %copy-done.13), channel_id=1, source_target_pairs={{0,1},{1,0},{2,3},{3,2},{4,5},{5,4},{6,7},{7,6},{8,9},{9,8},{10,11... | collective-permute-start | bytes 3080 | tf_op jit(solution)/shard_map/ppermute | solution.py:496
  86.1 9.1 %collective-permute-start.3 = (f32[128]{0:T(128)S(1)}, f32[128]{0:T(128)S(1)}, u32[]{:S(2)}, u32[]{:S(2)}) collective-permute-start(f32[128]{0:T(128)S(1)} %copy-done.14), channel_id=1, source_target_pairs={{0,1},{1,0},{2,3},{3,2},{4,5},{5,4},{6,7},{7,6},{8,9},{9,8},{10,11... | collective-permute-start | bytes 1544 | tf_op jit(solution)/shard_map/ppermute | solution.py:496
  86.2 4.6 %copy-start.11 = (bf16[4,4,4,2,128,384]{5,4,3,2,1,0:T(8,128)(2,1)S(1)}, bf16[4,4,4,2,128,384]{5,4,3,2,1,0:T(8,128)(2,1)}, u32[]{:S(2)}) copy-start(bf16[4,4,4,2,128,384]{5,4,3,2,1,0:T(8,128)(2,1)} %copy-done.10) | copy-start | bytes 37748740
  95.8 3.7 %copy-start.12 = (bf16[1024,2048]{1,0:T(8,128)(2,1)S(1)}, bf16[1024,2048]{1,0:T(8,128)(2,1)}, u32[]{:S(2)}) copy-start(bf16[1024,2048]{1,0:T(8,128)(2,1)} %param.25) | copy-start | bytes 12582916
  97.0 3.2 %copy-start = (bf16[128,2048]{1,0:T(8,128)(2,1)S(1)}, bf16[128,2048]{1,0:T(8,128)(2,1)}, u32[]{:S(2)}) copy-start(bf16[128,2048]{1,0:T(8,128)(2,1)} %residual_ref.1) | copy-start | bytes 1572868
  97.0 3.2 %copy-start.7 = (f32[2048]{0:T(1024)S(1)}, f32[2048]{0:T(1024)}, u32[]{:S(2)}) copy-start(f32[2048]{0:T(1024)} %param.26) | copy-start | bytes 24580
  97.0 3.2 %copy-start.8 = (f32[2048]{0:T(1024)S(1)}, f32[2048]{0:T(1024)}, u32[]{:S(2)}) copy-start(f32[2048]{0:T(1024)} %param.27) | copy-start | bytes 24580
  97.1 3.2 %copy-start.9 = (f32[2048]{0:T(1024)S(1)}, f32[2048]{0:T(1024)}, u32[]{:S(2)}) copy-start(f32[2048]{0:T(1024)} %param.28) | copy-start | bytes 24580

commit v3 on v2

v3 whole, which is shorter than its diff:
```python
import functools
import math

import jax
import jax.numpy as jnp
from jax import lax
from jax.experimental import pallas as pl
from jax.experimental.pallas import tpu as pltpu
from jax.sharding import PartitionSpec as P


MESH = pl.DeviceIdType.MESH
norm_eps = 1e-06
far_score = -1e30
log2e = 1.4426950408889634
f32, bf16 = jnp.float32, jnp.bfloat16
unit = 1024
own_units = 10

orders = (("x", "y", "z"), ("y", "z", "x"), ("z", "x", "y"))
pieces = (
    (0, 0, 0, 32, 16),
    (1, 0, 48, 32, 16),
    (2, 0, 96, 32, 16),
    (0, 0, 32, 16, 8),
    (1, 0, 80, 16, 8),
    (2, 1, 0, 32, 16),
)
shift = (3, 1, 2, 2)


def routing(ids_ref, bias_ref, table_ref, weight_ref, tp):
    expert = lax.broadcasted_iota(jnp.int32, (128, 128), 0)
    earlier = (expert < lax.broadcasted_iota(jnp.int32, (128, 128), 1)).astype(bf16)
    place = lax.broadcasted_iota(jnp.int32, (512, 128), 0)
    for core in range(2):
        table = jnp.zeros((512, 128), f32)
        weight = jnp.zeros((512, 128), f32)
        taken = jnp.zeros((128, 1), f32)
        for k in range(2):
            ids = ids_ref[core, k : k + 1, :]
            marked = (expert == ids).astype(f32)
            counts = jnp.dot(marked.astype(bf16), earlier, preferred_element_type=f32) + taken
            taken = taken + jnp.sum(marked, axis=1, keepdims=True)
            rank = jnp.sum(marked * counts, axis=0, keepdims=True).astype(jnp.int32)
            slot = jnp.where((ids & 1) == tp, (ids >> 1) * 8 + core * 4 + rank, -1)
            bias = bias_ref[core]
            share = 1.0 / (1.0 + jnp.exp(-bias if k == 0 else bias))
            here = place == slot
            table = jnp.where(here, 1.0, table)
            weight = jnp.where(here, share, weight)
        columns = slice(core * 128, core * 128 + 128)
        table_ref[:, columns] = table.astype(bf16)
        turned = weight.T
        high = turned.astype(bf16)
        weight_ref[columns, 0:512] = high
        weight_ref[columns, 512:1024] = (turned - high.astype(f32)).astype(bf16)


def gather_kernel(small_ref, large_ref, cum_s_ref, cum_l_ref, qs_ref, ql_ref, route_ref, bias_ref,
                  g_ref, c_ref, far_qs, far_ql, far_gates, table_ref, weight_ref, gates_ref,
                  ids, biases, own, own_sems, send, recv, dsend, drecv, far_send, far_recv, pair_send, pair_recv):
    sp, tp = lax.axis_index("sp"), lax.axis_index("tp")
    at = {"z": sp // 16, "y": (sp // 4) % 4, "x": sp % 4}
    partner = (sp, 1 - tp)
    mirror = (63 - sp, tp)
    far_qs[...] = jnp.zeros(far_qs.shape, bf16)
    far_ql[...] = jnp.zeros(far_ql.shape, bf16)
    far_gates[...] = jnp.zeros(far_gates.shape, f32)

    def moved(dim, by):
        here = dict(at)
        here[dim] = (at[dim] + by) % 4
        return (here["z"] * 16 + here["y"] * 4 + here["x"], tp)

    barrier = pltpu.get_barrier_semaphore()
    for dim in ("x", "y", "z"):
        for by in (1, 3):
            pl.semaphore_signal(barrier, inc=1, device_id=moved(dim, by), device_id_type=MESH)
    pl.semaphore_signal(barrier, inc=1, device_id=partner, device_id_type=MESH)
    pl.semaphore_signal(barrier, inc=1, device_id=mirror, device_id_type=MESH)

    gates_ref[...] = jnp.concatenate([cum_s_ref[...], cum_l_ref[...] * jnp.float32(math.sqrt(2.0)), jnp.zeros((4, 256), f32)], axis=0)
    staged, placed = [], []
    for half in (0, 1):
        rows = pl.ds(half * 128, 128)
        staged.append(pltpu.make_async_copy(small_ref.at[rows, :], own.at[half, :, pl.ds(0, 128)], own_sems.at[half]))
        staged.append(pltpu.make_async_copy(large_ref.at[rows, :], own.at[half, :, pl.ds(128, 256)], own_sems.at[2 + half]))
        placed.append(pltpu.make_async_copy(own.at[half], g_ref.at[at["z"], at["y"], at["x"], half], own_sems.at[4 + half]))
        c_ref[at["z"], at["y"], at["x"], half * 16 : half * 16 + 16, :] = gates_ref[:, half * 128 : half * 128 + 128]
    for copy in staged:
        copy.start()
    ids[tp] = route_ref[...]
    biases[tp] = bias_ref[...]
    pairs = [
        pltpu.make_async_remote_copy(
            src_ref=source, dst_ref=whole.at[tp], send_sem=pair_send.at[k], recv_sem=pair_recv.at[k],
            device_id=partner, device_id_type=MESH)
        for k, (source, whole) in enumerate(((route_ref, ids), (bias_ref, biases)))
    ]
    paired = [
        pltpu.make_async_remote_copy(
            src_ref=whole.at[1 - tp], dst_ref=whole.at[1 - tp], send_sem=pair_send.at[k], recv_sem=pair_recv.at[k],
            device_id=partner, device_id_type=MESH)
        for k, whole in enumerate((ids, biases))
    ]

    def rows_of(piece, kind):
        _, _, first, count, half = pieces[piece]
        if kind == 2:
            return (first, half)
        if kind == 3:
            return (first + half, count - half)
        return (first, count)

    def view(piece, phase, offset, kind, side):
        order = orders[pieces[piece][0]]
        index = []
        for dim in ("z", "y", "x"):
            where = order.index(dim)
            if where < phase:
                index.append(slice(None))
            else:
                index.append((at[dim] + offset) % 4 if where == phase else at[dim])
        rows = pl.ds(*rows_of(piece, kind))
        if pieces[piece][1]:
            return c_ref.at[(*index, rows, slice(None))]
        return g_ref.at[(*index, side, rows, slice(None))]

    def sent(piece, phase, kind):
        target = view(piece, phase, (0, 0, 3, 1)[kind], kind, tp)
        source = target
        if phase == 0 and kind < 2 and pieces[piece][1] == 0:
            source = own.at[tp, pl.ds(*rows_of(piece, kind)), :]
        return pltpu.make_async_remote_copy(
            src_ref=source, dst_ref=target, send_sem=send.at[piece, phase, kind], recv_sem=recv.at[piece, phase, kind],
            device_id=moved(orders[pieces[piece][0]][phase], 1 if kind in (0, 2) else 3), device_id_type=MESH)

    def arrived(piece, phase, kind):
        ref = view(piece, phase, shift[kind], kind, tp)
        return pltpu.make_async_remote_copy(
            src_ref=ref, dst_ref=ref, send_sem=send.at[piece, phase, kind], recv_sem=recv.at[piece, phase, kind],
            device_id=partner, device_id_type=MESH)

    def shared(piece, phase, kind, side):
        ref = view(piece, phase, shift[kind], kind, side)
        return pltpu.make_async_remote_copy(
            src_ref=ref, dst_ref=ref, send_sem=dsend.at[piece, phase, kind], recv_sem=drecv.at[piece, phase, kind],
            device_id=partner, device_id_type=MESH)

    far = [
        pltpu.make_async_remote_copy(
            src_ref=source, dst_ref=target, send_sem=far_send.at[k], recv_sem=far_recv.at[k],
            device_id=mirror, device_id_type=MESH)
        for k, (source, target) in enumerate(((gates_ref, far_gates), (qs_ref, far_qs), (ql_ref, far_ql)))
    ]
    count = range(len(pieces))
    for copy in staged:
        copy.wait()
    for copy in placed:
        copy.start()
    pl.semaphore_wait(barrier, 8)
    for piece in count:
        for kind in (0, 1):
            sent(piece, 0, kind).start()

    @pl.when(sp >= 32)
    def _():
        for copy in far:
            copy.start()

    for copy in pairs:
        copy.start()
    for copy in placed:
        copy.wait()
    for phase in range(3):
        if phase == 2:
            for copy in paired:
                copy.wait_recv()
            routing(ids, biases, table_ref, weight_ref, tp)
        for piece in count:
            for kind in (0, 1):
                arrived(piece, phase, kind).wait_recv()
                sent(piece, phase, 2 + kind).start()
                if pieces[piece][1] == 0:
                    shared(piece, phase, kind, tp).start()
        for piece in count:
            for kind in (2, 3):
                arrived(piece, phase, kind).wait_recv()
            if phase < 2:
                for kind in (0, 1):
                    sent(piece, phase + 1, kind).start()
            if pieces[piece][1] == 0:
                for kind in (2, 3):
                    shared(piece, phase, kind, tp).start()

    for copy in pairs:
        copy.wait_send()

    @pl.when(sp >= 32)
    def _():
        for copy in far:
            copy.wait_send()

    @pl.when(sp < 32)
    def _():
        for copy in far:
            copy.wait_recv()

    for phase in range(3):
        for piece in count:
            for kind in range(4):
                sent(piece, phase, kind).wait_send()
                if pieces[piece][1] == 0:
                    shared(piece, phase, kind, tp).wait_send()
                    shared(piece, phase, kind, 1 - tp).wait_recv()


def gather(small, large, cum_s, cum_l, qs, ql, route, bias):
    DMA = pltpu.SemaphoreType.DMA
    shape = (len(pieces), 3, 4)
    V = pl.BlockSpec(memory_space=pltpu.VMEM)
    A = pl.BlockSpec(memory_space=pl.ANY)
    return pl.pallas_call(
        gather_kernel,
        out_shape=(
            jax.ShapeDtypeStruct((4, 4, 4, 2, 128, 384), bf16),
            jax.ShapeDtypeStruct((4, 4, 4, 32, 128), f32),
            jax.ShapeDtypeStruct((256, 512), bf16),
            jax.ShapeDtypeStruct((256, 512), bf16),
            jax.ShapeDtypeStruct((16, 256), f32),
            jax.ShapeDtypeStruct((512, 256), bf16),
            jax.ShapeDtypeStruct((256, 1024), bf16),
            jax.ShapeDtypeStruct((16, 256), f32),
        ),
        in_specs=[A, A, V, V, A, A, V, V],
        out_specs=(A,) + (V,) * 7,
        scratch_shapes=[
            pltpu.VMEM((2, 2, 128), jnp.int32), pltpu.VMEM((2, 1, 128), f32), pltpu.VMEM((2, 128, 384), bf16), DMA((6,)),
            DMA(shape), DMA(shape), DMA(shape), DMA(shape), DMA((3,)), DMA((3,)), DMA((2,)), DMA((2,)),
        ],
        compiler_params=pltpu.CompilerParams(collective_id=0, has_side_effects=True, vmem_limit_bytes=60 * 1024 * 1024),
        name="gather_keys",
    )(small, large, cum_s, cum_l, qs, ql, route, bias)


def attention_kernel(qs_hbm, ql_hbm, cq_ref, whole_ref, c_ref, *refs, diagonal):
    if diagonal:
        o_ref, ml_ref, *scratch = refs
    else:
        (o_ref, *scratch), ml_ref = refs, None
    attend(qs_hbm, ql_hbm, cq_ref, whole_ref, c_ref, o_ref, ml_ref, *scratch, diagonal=diagonal)


def split3(values):
    high = values.astype(bf16).astype(f32)
    rest = values - high
    middle = rest.astype(bf16).astype(f32)
    return high, middle, rest - middle


def attend(qs_hbm, ql_hbm, cq_ref, whole_ref, c_ref, o_ref, ml_ref,
                     qs_ref, ql_ref, query_sems, near, near_sems, tile, vts, vtl, qs, ql, acc_s, acc_l, top, *, diagonal):
    sp = lax.axis_index("sp")
    if diagonal:
        hi, q0 = sp // 4 + 1, sp * 256
        lo = jnp.maximum(hi - own_units, 0)
    else:
        lo, q0 = 0, (63 - sp) * 256
        hi = jnp.where(sp < 32, jnp.maximum((63 - sp) // 4 + 1 - own_units, 0), 0)

    def fetch(i):
        return pltpu.make_async_copy(
            whole_ref.at[pl.ds(pl.multiple_of((hi - 1 - i) * unit, unit), unit), :], near.at[i], near_sems.at[i])

    n = hi - lo

    @pl.when(n > 0)
    def _():
        queries = [
            pltpu.make_async_copy(qs_hbm, qs_ref, query_sems.at[0]),
            pltpu.make_async_copy(ql_hbm, ql_ref, query_sems.at[1]),
        ]
        for copy in queries:
            copy.start()
        lax.fori_loop(0, hi - lo, lambda i, _: (fetch(i).start(), 0)[1], 0)
        nq = 256
        cs, cl = log2e / 8.0, log2e / math.sqrt(128.0)

        acc_s[...] = jnp.zeros(acc_s.shape, f32)
        acc_l[...] = jnp.zeros(acc_l.shape, f32)
        top[...] = jnp.zeros(top.shape, f32)
        vts[64:80, :] = jnp.ones((16, unit), bf16)
        vtl[128:144, :] = jnp.ones((16, unit), bf16)
        for copy in queries:
            copy.wait()
        for k in range(4):
            w = slice(k * nq, (k + 1) * nq)
            two = qs_ref[:, k * 128 : (k + 1) * 128].T
            qs[128:192, 2 * k * nq : (2 * k + 1) * nq] = two[0:64, :]
            qs[128:192, (2 * k + 1) * nq : (2 * k + 2) * nq] = two[64:128, :]
            ql[0:128, w] = ql_ref[:, k * 128 : (k + 1) * 128].T
        qs[192:256, :] = jnp.zeros((64, 2048), bf16)
        row = lax.broadcasted_iota(jnp.int32, (128, nq), 0)
        for h in range(12):
            here = cq_ref[h : h + 1, :]
            high = here.astype(bf16).astype(f32)
            rest = here - high
            middle = rest.astype(bf16).astype(f32)
            low = rest - middle
            chosen = jnp.where((row == h) | (row == 16 + h) | (row == 32 + h), -8.0, 0.0)
            chosen = jnp.where(row == 48, 8.0 * high, chosen)
            chosen = jnp.where(row == 49, 8.0 * middle, chosen)
            chosen = jnp.where(row == 50, 8.0 * low, chosen).astype(bf16)
            if h < 8:
                qs[0:128, h * nq : (h + 1) * nq] = chosen
            else:
                ql[128:256, (h - 8) * nq : (h - 7) * nq] = chosen
        size_s = jnp.max(jnp.sum(jnp.abs(qs[128:192, :].astype(f32)), axis=0, keepdims=True))
        size_l = jnp.max(jnp.sum(jnp.abs(ql[0:128, :].astype(f32)), axis=0, keepdims=True))
        bounded = (size_s <= 150.0) & (size_l <= 210.0)

        def ready(i):
            u = hi - 1 - i
            fetch(i).wait()
            here = near.at[i]
            for j in range(8):
                gate = c_ref[u * 4 + j // 2, (j % 2) * 16 : (j % 2) * 16 + 16, :]
                high = gate.astype(bf16).astype(f32)
                rest = gate - high
                middle = rest.astype(bf16).astype(f32)
                wide = jnp.concatenate([high, middle, rest - middle, jnp.ones((8, 128), f32), jnp.zeros((72, 128), f32)], axis=0)
                tile[j * 128 : (j + 1) * 128, :] = wide.T.astype(bf16)
            vts[0:64, :] = here[:, 0:128].T[64:128, :]
            vtl[0:128, :] = here[:, 256:384].T
            return u, here

        def keys_small(here):
            return jnp.concatenate([tile[...], here[:, 0:128]], axis=1)

        def keys_large(here):
            return jnp.concatenate([here[:, 128:256], tile[...]], axis=1)

        def allowed(u, width):
            key = u * unit + lax.broadcasted_iota(jnp.int32, (unit, width), 0)
            query = q0 + (lax.broadcasted_iota(jnp.int32, (unit, width), 1) & (nq - 1))
            return key <= query

        def quick(i, masked):
            u, here = ready(i)
            for keys, q, w, vt, acc, scale in (
                (keys_small, qs, 0, vts, acc_s, cs),
                (keys_small, qs, 1024, vts, acc_s, cs),
                (keys_large, ql, 0, vtl, acc_l, cl),
            ):
                s = jnp.dot(keys(here), q[:, w : w + 1024], preferred_element_type=f32) * scale
                if masked:
                    s = jnp.where(allowed(u, 1024), s, far_score)
                p = jnp.exp2(s).astype(bf16)
                acc[:, w : w + 1024] += jnp.dot(vt[...], p, preferred_element_type=f32)

        def careful(i, _):
            u, here = ready(i)

            def group(keys, q, vt, acc, scale, count, base):
                def head(h, _):
                    w = pl.ds(pl.multiple_of(h * nq, nq), nq)
                    s = jnp.dot(keys(here), q[:, w], preferred_element_type=f32) * scale
                    s = jnp.where(allowed(u, nq), s, far_score)
                    before = top[base + h]
                    after = jnp.maximum(before, jnp.max(s, axis=0, keepdims=True))
                    top[base + h] = after
                    p = jnp.exp2(s - after).astype(bf16)
                    acc[:, w] = acc[:, w] * jnp.exp2(before - after) + jnp.dot(vt[...], p, preferred_element_type=f32)
                    return 0

                lax.fori_loop(0, count, head, 0)

            group(keys_small, qs, vts, acc_s, cs, 8, 0)
            group(keys_large, ql, vtl, acc_l, cl, 4, 8)
            return 0

        @pl.when(bounded)
        def _():
            if diagonal:
                quick(0, True)
            lax.fori_loop(1 if diagonal else 0, n, lambda i, _: (quick(i, False), 0)[1], 0)

        @pl.when(jnp.logical_not(bounded))
        def _():
            top[...] = jnp.full(top.shape, far_score, f32)
            lax.fori_loop(0, n, careful, 0)

        tops, totals = [], []
        for h in range(12):
            size, acc, base, k = (64, acc_s, 0, h) if h < 8 else (128, acc_l, 512, h - 8)
            w = slice(k * nq, (k + 1) * nq)
            total = acc[size : size + 1, w]
            scale = jnp.where(total > 0, 1.0 / jnp.where(total > 0, total, 1.0), 0.0)
            o_ref[base + k * size : base + (k + 1) * size, :] = (acc[0:size, w] * scale).astype(o_ref.dtype)
            tops.append(top[h])
            totals.append(total)
        blank = jnp.zeros((4, nq), f32)
        ml = jnp.concatenate(tops + [blank] + totals + [blank], axis=0)
        if diagonal:
            ml_ref[...] = ml
        else:
            for k, piece in enumerate(split3(ml)):
                o_ref[1024 + 32 * k : 1056 + 32 * k, :] = piece.astype(bf16)

    @pl.when(n == 0)
    def _():
        o_ref[...] = jnp.zeros(o_ref.shape, o_ref.dtype)


def attention(qs, ql, cq, g, c, diagonal):
    V = pl.BlockSpec(memory_space=pltpu.VMEM)
    A = pl.BlockSpec(memory_space=pl.ANY)
    kind = f32 if diagonal else bf16
    VM = pltpu.VMEM
    return pl.pallas_call(
        functools.partial(attention_kernel, diagonal=diagonal),
        out_shape=(
            (jax.ShapeDtypeStruct((1024, 256), kind), jax.ShapeDtypeStruct((32, 256), f32))
            if diagonal
            else jax.ShapeDtypeStruct((1120, 256), kind)
        ),
        in_specs=[A, A, V, A, V],
        out_specs=(V, V) if diagonal else V,
        scratch_shapes=[
            VM((256, 512), bf16), VM((256, 512), bf16), pltpu.SemaphoreType.DMA((2,)),
            VM((own_units, unit, 384), bf16), pltpu.SemaphoreType.DMA((own_units,)), VM((unit, 128), bf16),
            VM((80, unit), bf16), VM((144, unit), bf16), VM((256, 2048), bf16), VM((256, 1024), bf16),
            VM((80, 2048), f32), VM((144, 1024), f32), VM((12, 1, 256), f32),
        ],
        compiler_params=pltpu.CompilerParams(vmem_limit_bytes=(52 if diagonal else 60) * 1024 * 1024),
        cost_estimate=pl.CostEstimate(flops=12_000_000_000 if diagonal else 8_000_000_000, bytes_accessed=12_000_000, transcendentals=26_000_000),
        name="attention_own" if diagonal else "attention_far",
    )(qs, ql, cq, g, c)


def reach(offset):
    return sum((0, 1, 2, 1)[(offset // step) % 4] for step in (1, 4, 16))


offsets = tuple(sorted(range(1, 64), key=lambda offset: -reach(offset)))


def expert_kernel(own_ref, far_ref, own_ml, small_hbm, large_hbm, residual_ref, mix_ref, route_ref, blend_ref, table_ref, weight_ref, gate_hbm, up_hbm, down_hbm, out_ref,
                  gate_w, up_w, down_w, project, part_ref, joined, other, rows, leaving, taken, hidden, made, back, kept, given, swapped,
                  load, pair_send, pair_recv, go_send, go_recv, back_send, back_recv):
    sp, tp = lax.axis_index("sp"), lax.axis_index("tp")
    z, y, x = sp // 16, (sp // 4) % 4, sp % 4

    def chip(offset, sign):
        oz, oy, ox = offset // 16, (offset // 4) % 4, offset % 4
        return ((z + sign * oz + 4) % 4) * 16 + ((y + sign * oy + 4) % 4) * 4 + (x + sign * ox + 4) % 4

    partner = (sp, 1 - tp)
    loads = [
        pltpu.make_async_copy(source.at[0], target, load.at[k])
        for k, (source, target) in enumerate(((gate_hbm, gate_w), (up_hbm, up_w), (down_hbm, down_w)))
    ]
    heads = pl.ds(pl.multiple_of(tp * 512, 512), 512)
    projections = [
        pltpu.make_async_copy(source.at[heads, :], project.at[pl.ds(512 * k, 512), :], load.at[3 + k])
        for k, source in enumerate((small_hbm, large_hbm))
    ]
    for copy in projections:
        copy.start()
    barrier = pltpu.get_barrier_semaphore()
    for offset in offsets:
        pl.semaphore_signal(barrier, inc=1, device_id=(chip(offset, 1), tp), device_id_type=MESH)
    pl.semaphore_signal(barrier, inc=1, device_id=partner, device_id_type=MESH)
    for copy in loads:
        copy.start()
    far_ml = sum(far_ref[1024 + 32 * k : 1056 + 32 * k, :].astype(f32) for k in range(3))
    for h in range(12):
        size, base = (64, h * 64) if h < 8 else (128, 512 + (h - 8) * 128)
        l_own, l_far = own_ml[16 + h : 17 + h, :], far_ml[16 + h : 17 + h, :]
        m_own = own_ml[h : h + 1, :]
        m_far = jnp.where(l_far > 0, far_ml[h : h + 1, :], far_score)
        most = jnp.maximum(m_own, m_far)
        a, b = l_own * jnp.exp2(m_own - most), l_far * jnp.exp2(m_far - most)
        whole = a + b
        rows_here = slice(base, base + size)
        joined[rows_here, :] = (own_ref[rows_here, :] * (a / whole) + far_ref[rows_here, :].astype(f32) * (b / whole)).astype(bf16)
    attended = joined[...].T
    for copy in projections:
        copy.wait()
    for w in range(0, 2048, 512):
        part_ref[:, w : w + 512] = jnp.dot(attended, project[:, w : w + 512], preferred_element_type=f32).astype(bf16)
    pl.semaphore_wait(barrier, 64)

    def across(source, target, k):
        return pltpu.make_async_remote_copy(
            src_ref=source, dst_ref=target, send_sem=pair_send.at[k], recv_sem=pair_recv.at[k],
            device_id=partner, device_id_type=MESH)

    first = across(part_ref.at[pl.ds((1 - tp) * 128, 128), :], other, 0)
    first.start()
    first.wait()

    def scaled(values, gain):
        return values * lax.rsqrt(jnp.mean(values * values, axis=-1, keepdims=True) + norm_eps) * gain

    mixer = part_ref[pl.ds(pl.multiple_of(tp * 128, 128), 128), :].astype(f32) + other[...].astype(f32)
    mixed = (residual_ref[...].astype(f32) + scaled(mixer, mix_ref[...])).astype(bf16)
    kept[...] = mixed
    given[...] = scaled(mixed.astype(f32), route_ref[...]).astype(bf16)
    mine = pl.ds(pl.multiple_of(tp * 128, 128), 128)
    rows[mine, :] = given[...]
    second = across(given, rows.at[mine, :], 1)
    second.start()
    second.wait_send()
    theirs = rows.at[pl.ds(pl.multiple_of((1 - tp) * 128, 128), 128), :]
    across(theirs, theirs, 1).wait_recv()
    for w in range(0, 2048, 512):
        leaving[:, :, w : w + 512] = jnp.dot(table_ref[...], rows[:, w : w + 512], preferred_element_type=f32).astype(bf16).reshape(64, 8, 512)

    def go(n):
        return pltpu.make_async_remote_copy(
            src_ref=leaving.at[chip(offsets[n], 1)], dst_ref=taken.at[n], send_sem=go_send.at[n], recv_sem=go_recv.at[n],
            device_id=(chip(offsets[n], 1), tp), device_id_type=MESH)

    def come(n):
        return pltpu.make_async_remote_copy(
            src_ref=made.at[n], dst_ref=back.at[sp], send_sem=back_send.at[n], recv_sem=back_recv.at[n],
            device_id=(chip(offsets[n], -1), tp), device_id_type=MESH)

    def came(n):
        ref = back.at[chip(offsets[n], 1)]
        return pltpu.make_async_remote_copy(
            src_ref=ref, dst_ref=ref, send_sem=back_send.at[n], recv_sem=back_recv.at[n], device_id=partner, device_id_type=MESH)

    for n in range(63):
        go(n).start()
    taken[63] = leaving[sp]
    for copy in loads:
        copy.wait()
    for group in (0, 1):
        members = range(32 * group, min(32 * group + 32, 63))
        for n in members:
            go(n).wait_recv()
        arrivals = taken[32 * group : 32 * group + 32].reshape(256, 2048)

        def widen(k, _):
            w = pl.ds(pl.multiple_of(k * 256, 256), 256)
            gated = jnp.dot(arrivals, gate_w[:, w], preferred_element_type=f32)
            upped = jnp.dot(arrivals, up_w[:, w], preferred_element_type=f32)
            hidden[:, w] = (gated / (1.0 + jnp.exp(-gated)) * upped).astype(bf16)
            return 0

        lax.fori_loop(0, 4, widen, 0)

        def narrow(k, _):
            w = pl.ds(pl.multiple_of(k * 512, 512), 512)
            made[32 * group : 32 * group + 32, :, w] = jnp.dot(hidden[...], down_w[:, w], preferred_element_type=f32).astype(bf16).reshape(32, 8, 512)
            return 0

        lax.fori_loop(0, 4, narrow, 0)
        for n in members:
            come(n).start()
    back[sp] = made[63]
    for n in range(63):
        go(n).wait_send()
    for n in range(63):
        came(n).wait_recv()
    for n in range(63):
        come(n).wait_send()
    ours = pl.ds(pl.multiple_of(tp * 128, 128), 128)
    away = pl.ds(pl.multiple_of((1 - tp) * 128, 128), 128)

    for w in range(0, 2048, 512):
        returned = back[:, :, w : w + 512].reshape(512, 512)
        given[:, w : w + 512] = (
            jnp.dot(weight_ref[away, 0:512], returned, preferred_element_type=f32)
            + jnp.dot(weight_ref[away, 512:1024], returned, preferred_element_type=f32)
        ).astype(bf16)
    third = across(given, swapped, 2)
    third.start()
    parts = []
    for w in range(0, 2048, 512):
        returned = back[:, :, w : w + 512].reshape(512, 512)
        parts.append(
            jnp.dot(weight_ref[ours, 0:512], returned, preferred_element_type=f32)
            + jnp.dot(weight_ref[ours, 512:1024], returned, preferred_element_type=f32)
        )
    third.wait()
    blended = jnp.concatenate(parts, axis=1) + swapped[...].astype(f32)
    out_ref[...] = (kept[...].astype(f32) + scaled(blended, blend_ref[...])).astype(bf16)


def experts(own_o, far_o, own_ml, out_small, out_large, residual, gain_mix, gain_route, gain_blend, table, weight, w_gate, w_up, w_down):
    V = pl.BlockSpec(memory_space=pltpu.VMEM)
    A = pl.BlockSpec(memory_space=pl.ANY)
    VM, DMA = pltpu.VMEM, pltpu.SemaphoreType.DMA
    return pl.pallas_call(
        expert_kernel,
        out_shape=jax.ShapeDtypeStruct((128, 2048), bf16),
        in_specs=[V] * 3 + [A] * 2 + [V] * 6 + [A] * 3,
        out_specs=V,
        scratch_shapes=[
            VM((2048, 1024), bf16), VM((2048, 1024), bf16), VM((1024, 2048), bf16),
            VM((1024, 2048), bf16), VM((256, 2048), bf16), VM((1024, 256), bf16),
            VM((128, 2048), bf16), VM((256, 2048), bf16), VM((64, 8, 2048), bf16), VM((64, 8, 2048), bf16),
            VM((256, 1024), bf16), VM((64, 8, 2048), bf16), VM((64, 8, 2048), bf16),
            VM((128, 2048), bf16), VM((128, 2048), bf16), VM((128, 2048), bf16),
            DMA((5,)), DMA((3,)), DMA((3,)), DMA((64,)), DMA((64,)), DMA((64,)), DMA((64,)),
        ],
        compiler_params=pltpu.CompilerParams(collective_id=1, has_side_effects=True, vmem_limit_bytes=50 * 1024 * 1024),
        name="experts",
    )(own_o, far_o, own_ml, out_small, out_large, residual, gain_mix, gain_route, gain_blend, table, weight, w_gate, w_up, w_down)


def on_device(
    queries_small,
    queries_large,
    kv_small,
    kv_large,
    cum_small,
    cum_large,
    residual,
    out_small,
    out_large,
    gain_mix,
    gain_route,
    gain_blend,
    w_gate,
    w_up,
    w_down,
    route,
    route_bias,
):
    chips = lax.axis_size("sp")
    to_late = [(i, chips - 1 - i) for i in range(chips // 2)]
    g, c, *far_q, table, weight, gates = gather(kv_small, kv_large, cum_small, cum_large, queries_small, queries_large, route, route_bias[None])
    g, c = g.reshape(chips * 256, 384), c.reshape(chips, 32, 128)
    far_o = attention(*far_q, g, c, False)
    far_o = lax.ppermute(far_o, "sp", to_late)
    own_o, own_ml = attention(queries_small, queries_large, gates, g, c, True)
    return experts(
        own_o, far_o, own_ml, out_small, out_large,
        residual, gain_mix[None], gain_route[None], gain_blend[None], table, weight, w_gate, w_up, w_down
    )


def solution(mesh):
    in_specs = (
        P("sp", "tp"),
        P("sp", "tp"),
        P("sp", None),
        P("sp", None),
        P("tp", "sp"),
        P("tp", "sp"),
        P(("sp", "tp"), None),
        P(),
        P(),
        P(),
        P(),
        P(),
        P(("sp", "tp"), None, None),
        P(("sp", "tp"), None, None),
        P(("sp", "tp"), None, None),
        P(None, ("sp", "tp")),
        P(("sp", "tp")),
    )
    out_specs = P(("sp", "tp"), None)
    return jax.shard_map(
        on_device, mesh=mesh, in_specs=in_specs, out_specs=out_specs, check_vma=False
    )
```

time: 226 us -> 222 us (0.982)
  local copies, waits for them, and re-layouts: 9.1 us -> 0.85 us
  Pallas kernels: 207 us -> 213 us
  waiting for transfers between devices: 0.67 us -> 5.98 us
  matrix products: 3.36 us -> 0 us
    unnamed x31 -> x19, local copies, waits for them, and re-layouts: 9.07 us -> 0.85 us
    ppermute x1, waiting for transfers between devices: 0.67 us -> 5.98 us  [on_device(): far_o = lax.ppermute(far_o, 'sp', to_late)]
    pallas_call x1, Pallas kernels: 55.5 us -> 59.7 us  [gather(): pl.pallas_call(gather_kernel, out_shape=(jax.ShapeDtypeStruct((4, 4, 4, 2...]
    dot_general x3 -> x0, matrix products: 3.36 us -> none  [the longest x1 2.38 us: on_device(): lax.dot_general(attn_small, weight_small, (((0,), (0,)), ((), ())), prefe...]
  transfers between devices with their start and end apart: 4 -> 1, of which waited for: 1 -> 1; matrix products, arithmetic and copies ran while one was open for 0% -> 0% of each run, Pallas kernels for 2% -> 3%
where the time goes in v3:
time: 222 us
  Pallas kernels  213 us (96%)
  waiting for transfers between devices  5.98 us (3%)
    pallas_call x1, Pallas kernels, experts(): pl.pallas_call(expert_kernel, out_shape=jax.ShapeDtypeStruct((128, 2048),...  125 us
    pallas_call x1, Pallas kernels, gather(): pl.pallas_call(gather_kernel, out_shape=(jax.ShapeDtypeStruct((4, 4, 4, 2...  59.7 us
    pallas_call x2, Pallas kernels, attention(): pl.pallas_call(functools.partial(attention_kernel, diagonal=diagonal), ou...  28.3 us
    ppermute x1, waiting for transfers between devices, on_device(): far_o = lax.ppermute(far_o, 'sp', to_late)  5.98 us
  transfers between devices with their start and end apart: 1, of which 1 were waited for; matrix products, arithmetic and copies ran while one was open for 0% of the time, Pallas kernels for 3%

profile of v3, /device:TPU:1, one launch (start us, length us, event | category | flops | bytes accessed | tf_op | source)
XLA Modules:
  0.0 221.5 jit_solution(11973299795109571385)
XLA Ops:
  0.0 59.7 %gather_keys.1 = (bf16[4,4,4,2,128,384]{5,4,3,2,1,0:T(8,128)(2,1)}, f32[4,4,4,32,128]{4,3,2,1,0:T(8,128)}, bf16[256,512]{1,0:T(8,128)(2,1)}, bf16[256,512]{1,0:T...) custom-call(bf16[256,128]{1,0:T(8,128)(2,1)} %small_ref.1, ...), custom_call_target="tpu_custom_call" | custom-call | tf_op jit(solution)/shard_map/gather_keys/pallas_call | solution.py:224
  59.7 0.0 copy-start.3
  59.7 0.0 copy-start.4
  59.7 0.0 copy-start.8
  59.7 21.6 %attention_far.1 = bf16[1120,256]{1,0:T(8,128)(2,1)} custom-call(bf16[256,512]{1,0:T(8,128)(2,1)} %get-tuple-element.19.qs_hbm, bf16[256,512]{1,0:T(8,128)(2,1)} %get-tuple-element.20.ql_hbm, f32[16,256]{1,0:T(8,128)} %get-tuple-element.21.cq_ref, bf16[16384,384]{1,0:T(8,128)(2,1)} %bitcast.10, f32[64,32,128]{2,1,0:T(8,128)} %bitcast.12), custom_call_target="tpu_custom_call" | custom-call | flops 8000000000 | bytes 12000000 | tf_op jit(solution)/shard_map/attention_far/pallas_call | solution.py:421
  81.4 1.3 collective-permute-start
  82.7 0.0 copy-done.3
  82.7 0.0 copy-done.4
  82.7 0.0 copy-done.8
  82.8 0.0 copy-start
  82.8 0.0 copy-start.1
  82.8 0.0 copy-start.2
  82.8 0.0 copy-start.5
  82.8 0.0 copy-start.6
  82.8 0.0 copy-start.7
  82.8 6.7 %attention_own.1 = (f32[1024,256]{1,0:T(8,128)S(1)}, f32[32,256]{1,0:T(8,128)S(1)}) custom-call(bf16[256,512]{1,0:T(8,128)(2,1)S(1)} %copy-done.3, bf16[256,512]{1,0:T(8,128)(2,1)S(1)} %copy-done.4, f32[16,256]{1,0:T(8,128)S(1)} %copy-done.8, bf16[16384,384]{1,0:T(8,128)(2,1)} %bitcast.11, f32[64,32,128]{2,1,0:T(8,128)} %bitcast.13), custom_call_target="tpu_custom_call" | custom-call | flops 12000000000 | bytes 12000000 | tf_op jit(solution)/shard_map/attention_own/pallas_call | solution.py:421
  89.5 6.0 %collective-permute-done.far_ref = bf16[1120,256]{1,0:T(8,128)(2,1)S(1)} collective-permute-done((bf16[1120,256]{1,0:T(8,128)(2,1)}, bf16[1120,256]{1,0:T(8,128)(2,1)S(1)}, u32[]{:S(2)}, u32[]{:S(2)}) %collective-permute-start) | collective-permute-done | bytes 573472 | tf_op jit(solution)/shard_map/ppermute | solution.py:640
  95.5 0.0 copy-done
  95.5 0.0 copy-done.1
  95.5 0.0 copy-done.2
  95.5 0.0 copy-done.5
  95.5 0.0 copy-done.6
  95.5 0.0 copy-done.7
  95.5 125.2 %experts.1 = bf16[128,2048]{1,0:T(8,128)(2,1)S(1)} custom-call(f32[1024,256]{1,0:T(8,128)S(1)} %get-tuple-element.18.own_ref, bf16[1120,256]{1,0:T(8,128)(2,1)S(1)} %collective-permute-done.far_ref, f32[32,256]{1,0:T(8,128)S(1)} %get-tuple-element.22.own_ml, bf16[1024,2048]{1,0:T(8,128)(2,1)} %small_hbm.1, bf16[1024,2048]{1,0:T(8,128)(2,1)} %large_hbm.1, ...), custom_call_target="tpu_custom_call" | custom-call | tf_op jit(solution)/shard_map/experts/pallas_call | solution.py:598
  220.7 0.8 copy.19
Async XLA Ops:
  59.7 23.0 %copy-start.3 = (bf16[256,512]{1,0:T(8,128)(2,1)S(1)}, bf16[256,512]{1,0:T(8,128)(2,1)}, u32[]{:S(2)}) copy-start(bf16[256,512]{1,0:T(8,128)(2,1)} %qs_hbm.1) | copy-start | bytes 786436
  59.7 23.0 %copy-start.4 = (bf16[256,512]{1,0:T(8,128)(2,1)S(1)}, bf16[256,512]{1,0:T(8,128)(2,1)}, u32[]{:S(2)}) copy-start(bf16[256,512]{1,0:T(8,128)(2,1)} %ql_hbm.1) | copy-start | bytes 786436
  59.7 23.0 %copy-start.8 = (f32[16,256]{1,0:T(8,128)S(1)}, f32[16,256]{1,0:T(8,128)}, u32[]{:S(2)}) copy-start(f32[16,256]{1,0:T(8,128)} %get-tuple-element.15.cq_ref) | copy-start | bytes 49156
  81.4 14.1 %collective-permute-start = (bf16[1120,256]{1,0:T(8,128)(2,1)}, bf16[1120,256]{1,0:T(8,128)(2,1)S(1)}, u32[]{:S(2)}, u32[]{:S(2)}) collective-permute-start(bf16[1120,256]{1,0:T(8,128)(2,1)} %attention_far.1), channel_id=1, source_target_pairs={{0,126},{2,124},{4,122},{6,120},{8,118},{10,116},{12,114},{14,112}... | collective-permute-start | bytes 1720328 | tf_op jit(solution)/shard_map/ppermute | solution.py:640
  82.8 12.7 %copy-start = (bf16[128,2048]{1,0:T(8,128)(2,1)S(1)}, bf16[128,2048]{1,0:T(8,128)(2,1)}, u32[]{:S(2)}) copy-start(bf16[128,2048]{1,0:T(8,128)(2,1)} %residual_ref.1) | copy-start | bytes 1572868
  82.8 12.7 %copy-start.1 = (bf16[256,1024]{1,0:T(8,128)(2,1)S(1)}, bf16[256,1024]{1,0:T(8,128)(2,1)}, u32[]{:S(2)}) copy-start(bf16[256,1024]{1,0:T(8,128)(2,1)} %get-tuple-element.24.weight_ref) | copy-start | bytes 1572868
  82.8 12.7 %copy-start.2 = (bf16[512,256]{1,0:T(8,128)(2,1)S(1)}, bf16[512,256]{1,0:T(8,128)(2,1)}, u32[]{:S(2)}) copy-start(bf16[512,256]{1,0:T(8,128)(2,1)} %get-tuple-element.23.table_ref) | copy-start | bytes 786436
  82.8 12.7 %copy-start.5 = (f32[2048]{0:T(1024)S(1)}, f32[2048]{0:T(1024)}, u32[]{:S(2)}) copy-start(f32[2048]{0:T(1024)} %param.26) | copy-start | bytes 24580
  82.8 12.7 %copy-start.6 = (f32[2048]{0:T(1024)S(1)}, f32[2048]{0:T(1024)}, u32[]{:S(2)}) copy-start(f32[2048]{0:T(1024)} %param.27) | copy-start | bytes 24580
  82.8 12.7 %copy-start.7 = (f32[2048]{0:T(1024)S(1)}, f32[2048]{0:T(1024)}, u32[]{:S(2)}) copy-start(f32[2048]{0:T(1024)} %param.28) | copy-start | bytes 24580
